TPU v7x, 32 devices: a whole 2x2x4 slice. The times are simulated.
32 devices in a mesh: kv: 8 (over z, y), tp: 4 (over x, core).
Axes of the slice: x: 2, y: 2, z: 4, core: 2. Of those that a mesh axis runs over, the one named last changes fastest.
Arguments:
- tokens: bfloat16 [32, 4096], P(None, 'kv'), may hold values from -40 to 40, as said below
- norm_gain: float32 [4096], P('kv'), may hold values from 0.1 to 1.9
- w_query: bfloat16 [4096, 2048], P('kv', 'tp'), may hold values from -0.09375 to 0.09375
- w_key: bfloat16 [4096, 512], P('kv', 'tp'), may hold values from -0.09375 to 0.09375
- w_value: bfloat16 [4096, 512], P('kv', 'tp'), may hold values from -0.09375 to 0.09375
- forget_weight: bfloat16 [4096, 32], replicated, may hold values from -0.09375 to 0.09375
- forget_bias: float32 [32], P('tp'), may hold values from -1 to 3
- kv_cache: bfloat16 [32, 10240, 8, 128], P(None, 'kv', 'tp'), may hold values from -6 to 6
- cum_gates: float32 [32, 32, 10240], P(None, 'tp', 'kv'), may hold values from -10500 to 0, as said below
- lengths: int32 [32], replicated, may hold values from 1 to 10240, as said below
- w_out: bfloat16 [2048, 4096], P('tp', 'kv'), may hold values from -0.25 to 0.25
Outputs:
- mixed: bfloat16 [32, 4096], P(None, 'kv')
- log_weight: float32 [32, 32], P(None, 'tp')
Inputs may be any that keep to these rules, and one draw needn't show every extreme that they name: Columns of tokens come in 16 groups of equal width. `cum_gates`: each row does not rise along the positions. `lengths`: some sequence has all 10240 positions cached.
All inputs are finite; a program needn't handle non-finite values.
Results may differ from a plain program's by a relative error of at most 0.0307.
Values may be sent and summed in bfloat16 or wider, within the bound.
A program may use at most 128 MiB of HBM per device.

v0:
```python
import functools
import jax
import jax.numpy as jnp
from jax import lax
from jax.experimental import pallas as pl
from jax.experimental.pallas import tpu as pltpu
from jax.sharding import PartitionSpec as P

norm_eps = 1e-05
masked_floor = -1e30
LANES = 128
MESH = pl.DeviceIdType.MESH


def flip(index, step, count):
    out = index
    bit = 1
    while bit < count:
        out = out + bit * ((step // bit) % 2) * (1 - 2 * ((index // bit) % 2))
        bit *= 2
    return out


def lane_of(shape):
    return lax.broadcasted_iota(jnp.int32, shape, len(shape) - 1)


def kernel(
    n_kv,
    n_tp,
    tokens_ref,
    gain_ref,
    bias_ref,
    lengths_ref,
    w_query_hbm,
    w_key_hbm,
    w_value_hbm,
    gate_hbm,
    cache_hbm,
    cum_hbm,
    w_out_hbm,
    mixed_ref,
    log_ref,
    w_query_ref,
    w_key_ref,
    w_value_ref,
    gate_ref,
    cache_ref,
    cum_ref,
    w_out_ref,
    shift_ref,
    last_ref,
    proj_ref,
    rs1_ref,
    query_ref,
    wide_ref,
    score_ref,
    peak_ref,
    own_query_ref,
    own_key_ref,
    own_value_ref,
    own_gate_ref,
    part_ref,
    rs2_ref,
    comb_ref,
    att_ref,
    rows_ref,
    tp_ref,
    weight_sems,
    cache_sems,
    rs1_send,
    rs1_recv,
    ag1_send,
    ag1_recv,
    rs2_send,
    rs2_recv,
    ag2_send,
    ag2_recv,
    tp_send,
    tp_recv,
):
    f32, bf16 = jnp.float32, jnp.bfloat16
    me = lax.axis_index("kv")
    my_tp = lax.axis_index("tp")
    rows, cols = tokens_ref.shape
    heads = cum_ref.shape[1]
    span = cum_ref.shape[2]
    kv_local = cache_ref.shape[1] // span
    group = heads // kv_local
    head_size = LANES // 2
    all_heads = gate_hbm.shape[0]
    mine = rows // n_kv
    q_cols = w_query_ref.shape[1]
    k_cols = w_key_ref.shape[1]
    k_pad = -(-k_cols // LANES) * LANES
    model_width = cols * n_kv
    inv_root = head_size ** (-0.5)

    gate_ref[...] = jnp.zeros_like(gate_ref)
    offset = pl.multiple_of(me * cols, cols)
    loads = [
        pltpu.make_async_copy(src, dst, weight_sems.at[i])
        for i, (src, dst) in enumerate(
            [
                (w_query_hbm, w_query_ref),
                (w_key_hbm, w_key_ref),
                (w_value_hbm, w_value_ref),
                (gate_hbm.at[:, pl.ds(offset, cols)], gate_ref.at[pl.ds(0, all_heads)]),
                (cum_hbm, cum_ref),
                (w_out_hbm, w_out_ref),
            ]
        )
    ]
    for load in loads[:5]:
        load.start()

    def cache_load(owner):
        at = pl.ds(owner * mine, mine)
        return pltpu.make_async_copy(cache_hbm.at[at], cache_ref.at[at], cache_sems.at[owner])

    barrier = pltpu.get_barrier_semaphore()
    for step in range(1, n_kv):
        pl.semaphore_signal(
            barrier, inc=1, device_id={"kv": flip(me, step, n_kv)}, device_id_type=MESH
        )
    for step in range(1, n_tp):
        pl.semaphore_signal(
            barrier, inc=1, device_id={"tp": flip(my_tp, step, n_tp)}, device_id_type=MESH
        )

    tokens_f = tokens_ref[...].astype(f32)
    squares = jnp.sum(tokens_f * tokens_f, axis=1, keepdims=True)
    normed = (tokens_f * gain_ref[...]).astype(bf16)
    for load in loads[:4]:
        load.wait()
    for step in range(n_kv):
        cache_load(flip(me, step, n_kv)).start()
    loads[5].start()
    pieces = [jnp.dot(normed, w_query_ref[...], preferred_element_type=f32)]
    for w_ref in (w_key_ref, w_value_ref):
        piece = jnp.dot(normed, w_ref[...], preferred_element_type=f32)
        if k_pad > k_cols:
            piece = jnp.concatenate([piece, jnp.zeros((rows, k_pad - k_cols), f32)], axis=1)
        pieces.append(piece)
    gates = lax.dot_general(
        normed, gate_ref[...], (((1,), (1,)), ((), ())), preferred_element_type=f32
    )
    pieces.append(jnp.where(lane_of(gates.shape) == all_heads, squares, gates))
    at = 0
    for piece in pieces:
        for owner in range(n_kv):
            proj_ref[owner, :, at : at + piece.shape[1]] = piece[
                owner * mine : (owner + 1) * mine
            ].astype(bf16)
        at += piece.shape[1]

    pl.semaphore_wait(barrier, n_kv + n_tp - 2)

    def rs1_copy(source, target):
        return pltpu.make_async_remote_copy(
            src_ref=proj_ref.at[target],
            dst_ref=rs1_ref.at[source],
            send_sem=rs1_send.at[target],
            recv_sem=rs1_recv.at[source],
            device_id={"kv": target},
            device_id_type=MESH,
        )

    for step in reversed(range(1, n_kv)):
        rs1_copy(me, flip(me, step, n_kv)).start()

    loads[4].wait()
    tile = (heads, LANES)
    lane = lane_of(tile)
    own_column = (lane % kv_local) == (lax.broadcasted_iota(jnp.int32, tile, 0) // group)

    def prepare(row, carry):
        length = lengths_ref[row] - me * span
        last = jnp.zeros(tile, f32)
        for chunk in range(span // LANES):
            cum = cum_ref[row, :, chunk * LANES : (chunk + 1) * LANES]
            place = lane + chunk * LANES
            shift = jnp.where(place < length, -cum, masked_floor)
            last = last + jnp.where(place == length - 1, cum, 0.0)
            for part in range(kv_local):
                if kv_local == 1:
                    spread = shift
                else:
                    pick = lane // kv_local + part * (LANES // kv_local)
                    spread = jnp.take_along_axis(shift, pick, axis=1)
                    spread = jnp.where(own_column, spread, masked_floor)
                at = (chunk * kv_local + part) * LANES
                shift_ref[row, :, at : at + LANES] = spread
        last_ref[row] = jnp.broadcast_to(jnp.sum(last, axis=1, keepdims=True), tile)
        return carry

    lax.fori_loop(0, rows, prepare, 0, unroll=4)

    total = proj_ref[me].astype(f32)
    for step in range(1, n_kv):
        other = flip(me, step, n_kv)
        rs1_copy(other, me).wait_recv()
        total = total + rs1_ref[other].astype(f32)
    misc = total[:, q_cols + 2 * k_pad :]
    misc_lane = lane_of(misc.shape)
    total_sq = jnp.sum(jnp.where(misc_lane == all_heads, misc, 0.0), axis=1, keepdims=True)
    row_scale = lax.rsqrt(total_sq / model_width + norm_eps)
    query_ref[me] = (row_scale * total[:, :q_cols]).astype(bf16)

    def ag1_copy(source, target):
        return pltpu.make_async_remote_copy(
            src_ref=query_ref.at[source],
            dst_ref=query_ref.at[source],
            send_sem=ag1_send.at[target],
            recv_sem=ag1_recv.at[source],
            device_id={"kv": target},
            device_id_type=MESH,
        )

    for step in reversed(range(1, n_kv)):
        ag1_copy(me, flip(me, step, n_kv)).start()

    part_lane = lane_of((mine, LANES))

    def spread_heads(ref, values, which, upper):
        for head in range(heads):
            at = which(head)
            pair = values[:, (at // 2) * LANES : (at // 2 + 1) * LANES]
            if (at % 2 == 1) != upper:
                pair = pltpu.roll(pair, head_size, 1)
            keep = (part_lane >= head_size) if upper else (part_lane < head_size)
            ref[pl.ds(head, mine, stride=heads), :] = jnp.where(keep, pair, 0.0)

    new_kv = (row_scale * total[:, q_cols : q_cols + 2 * k_pad]).astype(bf16).astype(f32)
    spread_heads(own_query_ref, query_ref[me].astype(f32), lambda head: head, False)
    spread_heads(own_key_ref, new_kv[:, :k_pad], lambda head: head // group, False)
    spread_heads(own_value_ref, new_kv[:, k_pad:], lambda head: head // group, True)
    for head in range(heads):
        own_gate_ref[pl.ds(head, mine, stride=heads), :] = row_scale * misc

    def rs2_copy(source, target):
        return pltpu.make_async_remote_copy(
            src_ref=part_ref.at[target],
            dst_ref=rs2_ref.at[source],
            send_sem=rs2_send.at[target],
            recv_sem=rs2_recv.at[source],
            device_id={"kv": target},
            device_id_type=MESH,
        )

    length_cols = cache_ref.shape[1]
    chunk_cols = 2 * LANES
    chunks = range(0, length_cols, chunk_cols)
    zeros = jnp.zeros((heads, LANES), f32)
    pairs = range(mine // 2)

    def entries(row_a, row_b, at):
        inside = slice(at, at + chunk_cols)
        return jnp.concatenate([cache_ref[row_a, inside, :], cache_ref[row_b, inside, :]], axis=1)

    def weigh(pair):
        peak = peak_ref[pair, :, :1]
        sums = jnp.zeros((2 * heads, chunk_cols), f32)
        weights = []
        for at in chunks:
            weight = jnp.exp(score_ref[pair, :, at : at + chunk_cols] - peak)
            sums = sums + weight
            weights.append(weight.astype(bf16))
        return weights, jnp.sum(sums, axis=1, keepdims=True), peak

    def score(owner, pair):
        first, second = 2 * pair, 2 * pair + 1
        row_a, row_b = owner * mine + first, owner * mine + second
        left = wide_ref[first * heads : (first + 1) * heads, :]
        right = wide_ref[second * heads : (second + 1) * heads, :]
        queries = jnp.concatenate(
            [
                jnp.concatenate([left, zeros], axis=1),
                jnp.concatenate([zeros, right], axis=1),
            ],
            axis=0,
        ).astype(bf16)
        peak = None
        for at in chunks:
            part = lax.dot_general(
                queries,
                entries(row_a, row_b, at),
                (((1,), (1,)), ((), ())),
                preferred_element_type=f32,
            )
            part = part + jnp.concatenate(
                [shift_ref[row_a, :, at : at + chunk_cols], shift_ref[row_b, :, at : at + chunk_cols]],
                axis=0,
            )
            score_ref[pair, :, at : at + chunk_cols] = part
            peak = part if peak is None else jnp.maximum(peak, part)
        peak_ref[pair] = jnp.broadcast_to(
            jnp.max(peak, axis=1, keepdims=True), (2 * heads, LANES)
        )

    def gather(owner, pair, weights, total_weight, peak):
        first, second = 2 * pair, 2 * pair + 1
        row_a, row_b = owner * mine + first, owner * mine + second
        values = jnp.zeros((2 * heads, chunk_cols), f32)
        for weight, at in zip(weights, chunks):
            values = values + jnp.dot(
                weight, entries(row_a, row_b, at), preferred_element_type=f32
            )
        for i, (place, row) in enumerate(((first, row_a), (second, row_b))):
            inside = slice(i * heads, (i + 1) * heads)
            out = values[inside, i * LANES : (i + 1) * LANES]
            out = jnp.where(lane == 0, peak[inside], out)
            out = jnp.where(lane == 1, total_weight[inside], out)
            out = jnp.where(lane == 2, last_ref[row], out)
            part_ref[owner, place * heads : (place + 1) * heads, :] = out

    def ready(owner):
        cache_load(owner).wait()
        spread_heads(wide_ref, query_ref[owner].astype(f32) * inv_root, lambda head: head, False)

    ready(me)
    for pair in pairs:
        score(me, pair)

    def attend(step, carry):
        owner, after = flip(me, step, n_kv), flip(me, step + 1, n_kv)
        ag1_copy(after, me).wait_recv()
        ready(after)
        for pair in pairs:
            weights = weigh(pair)
            score(after, pair)
            gather(owner, pair, *weights)

        @pl.when(step > 0)
        def _():
            rs2_copy(me, owner).start()

        return carry

    lax.fori_loop(0, n_kv - 1, attend, 0)
    final = flip(me, n_kv - 1, n_kv)
    for pair in pairs:
        gather(final, pair, *weigh(pair))
    rs2_copy(me, final).start()

    tall = (mine * heads, LANES)
    tall_lane = lane_of(tall)
    head_of = lax.broadcasted_iota(jnp.int32, tall, 0) % heads
    gate = jnp.sum(
        jnp.where(tall_lane == my_tp * heads + head_of, own_gate_ref[...], 0.0),
        axis=1,
        keepdims=True,
    )
    short = (mine * heads, heads)
    gate_bias = jnp.sum(
        jnp.where(
            lane_of(short) == lax.broadcasted_iota(jnp.int32, short, 0) % heads,
            jnp.broadcast_to(bias_ref[...], short),
            0.0,
        ),
        axis=1,
        keepdims=True,
    )
    gate = gate + gate_bias
    log_gate = jnp.minimum(gate, 0.0) - jnp.log1p(jnp.exp(-jnp.abs(gate)))
    new_score = (
        jnp.sum(own_query_ref[...] * own_key_ref[...], axis=1, keepdims=True) * inv_root
    )
    blocks = [part_ref[me]]
    for step in range(1, n_kv):
        other = flip(me, step, n_kv)
        rs2_copy(other, me).wait_recv()
        blocks.append(rs2_ref[other])
    last = blocks[0]
    for block in blocks[1:]:
        last = last + block
    cum_query = last[:, 2:3] + log_gate
    new_biased = new_score - cum_query
    peak = blocks[0]
    for block in blocks[1:]:
        peak = jnp.maximum(peak, block)
    peak = jnp.maximum(peak[:, 0:1], new_biased)
    new_weight = jnp.exp(new_biased - peak)
    values = new_weight.astype(bf16).astype(f32) * own_value_ref[...]
    for block in blocks:
        values = values + jnp.exp(block[:, 0:1] - peak) * block
    weight_sum = values[:, 1:2] + new_weight
    log_weight = peak + jnp.log(weight_sum) + cum_query
    comb_ref[...] = jnp.where(tall_lane < head_size, log_weight, values / weight_sum)

    tail = jnp.zeros((mine, LANES), f32)
    even = None
    for head in range(heads):
        row = comb_ref[pl.ds(head, mine, stride=heads), :]
        tail = jnp.where((part_lane == head) | (part_lane == heads + head), row, tail)
        if head % 2 == 0:
            even = pltpu.roll(row, head_size, 1)
        else:
            at = (head // 2) * LANES
            att_ref[me, :, at : at + LANES] = jnp.where(
                part_lane < head_size, even, row
            ).astype(bf16)
    coarse = tail.astype(bf16).astype(f32)
    att_ref[me, :, q_cols:] = jnp.where(part_lane < heads, coarse, tail - coarse).astype(bf16)

    def ag2_copy(source, target):
        return pltpu.make_async_remote_copy(
            src_ref=att_ref.at[source],
            dst_ref=att_ref.at[source],
            send_sem=ag2_send.at[target],
            recv_sem=ag2_recv.at[source],
            device_id={"kv": target},
            device_id_type=MESH,
        )

    for step in reversed(range(1, n_kv)):
        ag2_copy(me, flip(me, step, n_kv)).start()
    loads[5].wait()
    for step in range(1, n_kv):
        ag2_copy(flip(me, step, n_kv), me).wait_recv()
    for owner in range(n_kv):
        rows_ref[owner * mine : (owner + 1) * mine, :] = att_ref[owner].astype(f32)
    attended = rows_ref[:, :q_cols].astype(bf16)
    tp_ref[my_tp] = jnp.dot(attended, w_out_ref[...], preferred_element_type=f32).astype(bf16)

    def tp_copy(source, target):
        return pltpu.make_async_remote_copy(
            src_ref=tp_ref.at[source],
            dst_ref=tp_ref.at[source],
            send_sem=tp_send.at[target],
            recv_sem=tp_recv.at[source],
            device_id={"tp": target},
            device_id_type=MESH,
        )

    for step in reversed(range(1, n_tp)):
        tp_copy(my_tp, flip(my_tp, step, n_tp)).start()
    tails = rows_ref[:, q_cols:]
    log_ref[...] = tails[:, :heads] + tails[:, heads : 2 * heads]

    for step in range(1, n_kv):
        other = flip(me, step, n_kv)
        rs1_copy(me, other).wait_send()
        ag1_copy(me, other).wait_send()
        rs2_copy(me, other).wait_send()
        ag2_copy(me, other).wait_send()
    for step in range(1, n_tp):
        tp_copy(flip(my_tp, step, n_tp), my_tp).wait_recv()
    mixed = tp_ref[0].astype(f32)
    for source in range(1, n_tp):
        mixed = mixed + tp_ref[source].astype(f32)
    mixed_ref[...] = mixed.astype(bf16)
    for step in range(1, n_tp):
        tp_copy(my_tp, flip(my_tp, step, n_tp)).wait_send()


def shards(
    tokens,
    norm_gain,
    w_query,
    w_key,
    w_value,
    forget_weight,
    forget_bias,
    kv_cache,
    cum_gates,
    lengths,
    w_out,
):
    n_kv, n_tp = lax.axis_size("kv"), lax.axis_size("tp")
    rows, cols = tokens.shape
    span, kv_local, entry = kv_cache.shape[1:]
    heads = cum_gates.shape[1]
    q_cols, k_cols = w_query.shape[1], w_key.shape[1]
    k_pad = -(-k_cols // LANES) * LANES
    wide = q_cols + 2 * k_pad + LANES
    mine = rows // n_kv
    out_cols = w_out.shape[1]
    f32, bf16 = jnp.float32, jnp.bfloat16
    vmem = pl.BlockSpec(memory_space=pltpu.VMEM)
    smem = pl.BlockSpec(memory_space=pltpu.SMEM)
    hbm = pl.BlockSpec(memory_space=pl.ANY)
    dma = pltpu.SemaphoreType.DMA
    tall = (mine * heads, LANES)
    return pl.pallas_call(
        functools.partial(kernel, n_kv, n_tp),
        out_shape=(
            pltpu.VMEM((rows, out_cols), bf16),
            pltpu.VMEM((rows, heads), f32),
        ),
        in_specs=[vmem, vmem, vmem, smem] + [hbm] * 7,
        out_specs=(vmem, vmem),
        scratch_shapes=[
            pltpu.VMEM(w_query.shape, bf16),
            pltpu.VMEM(w_key.shape, bf16),
            pltpu.VMEM(w_value.shape, bf16),
            pltpu.VMEM((LANES, cols), bf16),
            pltpu.VMEM((rows, span * kv_local, entry), bf16),
            pltpu.VMEM(cum_gates.shape, f32),
            pltpu.VMEM(w_out.shape, bf16),
            pltpu.VMEM((rows, heads, span * kv_local), f32),
            pltpu.VMEM((rows, heads, LANES), f32),
            pltpu.VMEM((n_kv, mine, wide), bf16),
            pltpu.VMEM((n_kv, mine, wide), bf16),
            pltpu.VMEM((n_kv, mine, q_cols), bf16),
            pltpu.VMEM(tall, f32),
            pltpu.VMEM((mine // 2, 2 * heads, span * kv_local), f32),
            pltpu.VMEM((mine // 2, 2 * heads, LANES), f32),
            pltpu.VMEM(tall, f32),
            pltpu.VMEM(tall, f32),
            pltpu.VMEM(tall, f32),
            pltpu.VMEM(tall, f32),
            pltpu.VMEM((n_kv,) + tall, f32),
            pltpu.VMEM((n_kv,) + tall, f32),
            pltpu.VMEM(tall, f32),
            pltpu.VMEM((n_kv, mine, q_cols + LANES), bf16),
            pltpu.VMEM((rows, q_cols + LANES), f32),
            pltpu.VMEM((n_tp, rows, out_cols), bf16),
            dma((6,)),
            dma((n_kv,)),
        ]
        + [dma((n_kv,))] * 8
        + [dma((n_tp,))] * 2,
        compiler_params=pltpu.CompilerParams(
            collective_id=0, has_side_effects=True, vmem_limit_bytes=56 * 1024 * 1024
        ),
    )(
        tokens,
        norm_gain.reshape(1, cols),
        forget_bias.reshape(1, heads),
        lengths,
        w_query,
        w_key,
        w_value,
        forget_weight.T,
        kv_cache.reshape(rows, span * kv_local, entry),
        cum_gates,
        w_out,
    )


def solution(mesh):
    placed = (
        P(None, "kv"),
        P("kv"),
        P("kv", "tp"),
        P("kv", "tp"),
        P("kv", "tp"),
        P(),
        P("tp"),
        P(None, "kv", "tp", None),
        P(None, "tp", "kv"),
        P(),
        P("tp", "kv"),
    )
    return jax.shard_map(
        shards,
        mesh=mesh,
        in_specs=placed,
        out_specs=(P(None, "kv"), P(None, "tp")),
        check_vma=False,
    )
```

profile of v0, /device:TPU:0, one launch (start us, length us, event | category | flops | bytes accessed | tf_op | source)
XLA Modules:
  0.0 36.9 jit_solution(6858906360760710300)
XLA Ops:
  0.6 35.0 %shard_map.122 = (bf16[32,512]{1,0:T(8,128)(2,1)S(1)}, f32[32,8]{1,0:T(8,128)S(1)}) custom-call(bf16[32,512]{1,0:T(8,128)(2,1)} %tokens_ref.1, f32[1,512]{1,0:T(1,128)} %bitcast.6, f32[1,8]{1,0:T(1,128)} %bitcast.7, s32[32]{0:T(128)} %lengths_ref.1, bf16[512,512]{1,0:T(8,128)(2,1)} %w_query_hbm.1, bf16[512,128]{1,0:T(8,128)(2,1)} %w_key_hbm.1, ...), custom_call_target="tpu_custom_call" | custom-call | tf_op jit(solution)/shard_map/pallas_call | solution.py:485
  35.6 0.6 %copy.15 = bf16[32,512]{1,0:T(8,128)(2,1)} copy(bf16[32,512]{1,0:T(8,128)(2,1)S(1)} %get-tuple-element.4) | data formatting | bytes 65536
  36.2 0.7 %copy.13 = f32[32,8]{0,1:T(8,128)} copy(f32[32,8]{1,0:T(8,128)S(1)} %get-tuple-element.3) | data formatting | bytes 2048 | tf_op jit(solution)/shard_map/pallas_call | solution.py:485
where the time goes:
time: 37.1 us; the launch traced here: 36.9 us
  Pallas kernels  35 us (94%)
  local copies, waits for them, and re-layouts  1.28 us (3%)
  between operations  0.64 us (2%)
    pallas_call x1, Pallas kernels, shards(): pl.pallas_call(functools.partial(kernel, n_kv, n_tp), out_shape=(pltpu.VM...  35 us

commit v1 on v0

v1 whole, which is shorter than its diff:
```python
import functools
import jax
import jax.numpy as jnp
from jax import lax
from jax.experimental import pallas as pl
from jax.experimental.pallas import tpu as pltpu
from jax.sharding import PartitionSpec as P

norm_eps = 1e-05
masked_floor = -1e30
LANES = 128
MESH = pl.DeviceIdType.MESH


def flip(index, step, count):
    out = index
    bit = 1
    while bit < count:
        out = out + bit * ((step // bit) % 2) * (1 - 2 * ((index // bit) % 2))
        bit *= 2
    return out


def lane_of(shape):
    return lax.broadcasted_iota(jnp.int32, shape, len(shape) - 1)


def kernel(
    n_kv,
    n_tp,
    tokens_ref,
    gain_ref,
    bias_ref,
    lengths_ref,
    w_query_hbm,
    w_key_hbm,
    w_value_hbm,
    gate_hbm,
    cache_hbm,
    cum_hbm,
    w_out_hbm,
    mixed_ref,
    log_ref,
    w_query_ref,
    w_key_ref,
    w_value_ref,
    gate_ref,
    cache_ref,
    cum_ref,
    w_out_ref,
    shift_ref,
    last_ref,
    proj_ref,
    rs1_ref,
    query_ref,
    new_ref,
    bias_pad_ref,
    wide_ref,
    score_ref,
    peak_ref,
    value_ref,
    stat_ref,
    part_ref,
    gathered_ref,
    fresh_ref,
    order_ref,
    wide_rows_ref,
    tp_ref,
    weight_sems,
    cache_sems,
    rs1_send,
    rs1_recv,
    ag1_send,
    ag1_recv,
    new_send,
    new_recv,
    part_send,
    part_recv,
    tp_send,
    tp_recv,
):
    f32, bf16 = jnp.float32, jnp.bfloat16
    me = lax.axis_index("kv")
    my_tp = lax.axis_index("tp")
    rows, cols = tokens_ref.shape
    heads = cum_ref.shape[1]
    span = cum_ref.shape[2]
    entries = cache_ref.shape[1]
    kv_local = entries // span
    group = heads // kv_local
    head_size = LANES // 2
    all_heads = gate_hbm.shape[0]
    mine = rows // n_kv
    pairs = mine // 2
    tall = mine * heads
    q_cols = w_query_ref.shape[1]
    k_cols = w_key_ref.shape[1]
    k_pad = -(-k_cols // LANES) * LANES
    model_width = cols * n_kv
    inv_root = head_size ** (-0.5)
    chunk_cols = 2 * LANES
    chunks = range(0, entries, chunk_cols)
    segment = LANES // 4

    gate_ref[...] = jnp.zeros_like(gate_ref)
    offset = pl.multiple_of(me * cols, cols)
    loads = [
        pltpu.make_async_copy(src, dst, weight_sems.at[i])
        for i, (src, dst) in enumerate(
            [
                (w_query_hbm, w_query_ref),
                (w_key_hbm, w_key_ref),
                (w_value_hbm, w_value_ref),
                (gate_hbm.at[:, pl.ds(offset, cols)], gate_ref.at[pl.ds(0, all_heads)]),
                (cum_hbm, cum_ref),
                (w_out_hbm, w_out_ref),
            ]
        )
    ]
    for load in loads[:5]:
        load.start()

    def cache_load(owner):
        at = pl.ds(owner * mine, mine)
        return pltpu.make_async_copy(cache_hbm.at[at], cache_ref.at[at], cache_sems.at[owner])

    barrier = pltpu.get_barrier_semaphore()
    for step in range(1, n_kv):
        pl.semaphore_signal(
            barrier, inc=1, device_id={"kv": flip(me, step, n_kv)}, device_id_type=MESH
        )
    for step in range(1, n_tp):
        pl.semaphore_signal(
            barrier, inc=1, device_id={"tp": flip(my_tp, step, n_tp)}, device_id_type=MESH
        )

    tokens_f = tokens_ref[...].astype(f32)
    squares = jnp.sum(tokens_f * tokens_f, axis=1, keepdims=True)
    normed = (tokens_f * gain_ref[...]).astype(bf16)
    bias_pad_ref[...] = jnp.zeros_like(bias_pad_ref)
    bias_pad_ref[:, 0:heads] = bias_ref[...]
    for load in loads[:4]:
        load.wait()
    for step in range(n_kv):
        cache_load(flip(me, step, n_kv)).start()
    loads[5].start()
    pieces = [jnp.dot(normed, w_query_ref[...], preferred_element_type=f32)]
    for w_ref in (w_key_ref, w_value_ref):
        piece = jnp.dot(normed, w_ref[...], preferred_element_type=f32)
        if k_pad > k_cols:
            piece = jnp.concatenate([piece, jnp.zeros((rows, k_pad - k_cols), f32)], axis=1)
        pieces.append(piece)
    gates = lax.dot_general(
        normed, gate_ref[...], (((1,), (1,)), ((), ())), preferred_element_type=f32
    )
    pieces.append(jnp.where(lane_of(gates.shape) == all_heads, squares, gates))
    at = 0
    for piece in pieces:
        for owner in range(n_kv):
            proj_ref[owner, :, at : at + piece.shape[1]] = piece[
                owner * mine : (owner + 1) * mine
            ].astype(bf16)
        at += piece.shape[1]

    def rs1_copy(source, target):
        return pltpu.make_async_remote_copy(
            src_ref=proj_ref.at[target],
            dst_ref=rs1_ref.at[source],
            send_sem=rs1_send.at[target],
            recv_sem=rs1_recv.at[source],
            device_id={"kv": target},
            device_id_type=MESH,
        )

    pl.semaphore_wait(barrier, n_kv + n_tp - 2)
    for step in reversed(range(1, n_kv)):
        rs1_copy(me, flip(me, step, n_kv)).start()

    loads[4].wait()
    tile = (heads, LANES)
    lane = lane_of(tile)
    own_column = (lane % kv_local) == (lax.broadcasted_iota(jnp.int32, tile, 0) // group)

    def prepare(row, carry):
        length = lengths_ref[row] - me * span
        last = jnp.zeros(tile, f32)
        for chunk in range(span // LANES):
            cum = cum_ref[row, :, chunk * LANES : (chunk + 1) * LANES]
            place = lane + chunk * LANES
            shift = jnp.where(place < length, -cum, masked_floor)
            last = last + jnp.where(place == length - 1, cum, 0.0)
            for part in range(kv_local):
                if kv_local == 1:
                    spread = shift
                else:
                    pick = lane // kv_local + part * (LANES // kv_local)
                    spread = jnp.take_along_axis(shift, pick, axis=1)
                    spread = jnp.where(own_column, spread, masked_floor)
                at = (chunk * kv_local + part) * LANES
                shift_ref[row, :, at : at + LANES] = spread
        last_ref[row] = jnp.broadcast_to(jnp.sum(last, axis=1, keepdims=True), tile)
        return carry

    lax.fori_loop(0, rows, prepare, 0, unroll=4)

    piece_rows = LANES
    narrow = lane_of((piece_rows, LANES)) < head_size

    def pack(owner):
        cache_load(owner).wait()

        def body(i, carry):
            inside = pl.ds(pl.multiple_of(i * piece_rows, piece_rows), piece_rows)
            for pair in range(pairs):
                row = owner * mine + 2 * pair
                first, second = cache_ref[row, inside, :], cache_ref[row + 1, inside, :]
                turned = pltpu.roll(second, head_size, 1)
                cache_ref[row, inside, :] = jnp.where(narrow, first, turned)
                cache_ref[row + 1, inside, :] = jnp.where(narrow, turned, first)
            return carry

        lax.fori_loop(0, entries // piece_rows, body, 0, unroll=2)

    def pack_step(step, carry):
        pack(flip(me, step, n_kv))
        return carry

    lax.fori_loop(0, n_kv, pack_step, 0)

    total = proj_ref[me].astype(f32)
    for step in range(1, n_kv):
        other = flip(me, step, n_kv)
        rs1_copy(other, me).wait_recv()
        total = total + rs1_ref[other].astype(f32)
    misc = total[:, q_cols + 2 * k_pad :]
    part_lane = lane_of((mine, LANES))
    total_sq = jnp.sum(jnp.where(part_lane == all_heads, misc, 0.0), axis=1, keepdims=True)
    row_scale = lax.rsqrt(total_sq / model_width + norm_eps)
    query_ref[me] = (row_scale * total[:, :q_cols]).astype(bf16)

    def ag1_copy(source, target):
        return pltpu.make_async_remote_copy(
            src_ref=query_ref.at[source],
            dst_ref=query_ref.at[source],
            send_sem=ag1_send.at[target],
            recv_sem=ag1_recv.at[source],
            device_id={"kv": target},
            device_id_type=MESH,
        )

    for step in reversed(range(1, n_kv)):
        ag1_copy(me, flip(me, step, n_kv)).start()

    low_half = part_lane < head_size
    even_row = lax.broadcasted_iota(jnp.int32, (mine, LANES), 0) % 2 == 0

    def grouped(values, width):
        tiles = []
        for at in range(0, width, LANES):
            halves = []
            for half in range(2):
                source = (at // head_size + half) // group
                found = values[:, (source // 2) * LANES : (source // 2 + 1) * LANES]
                if source % 2 != half:
                    found = pltpu.roll(found, head_size, 1)
                halves.append(found)
            low = lane_of(halves[0].shape) < head_size
            tiles.append(jnp.where(low, halves[0], halves[1]))
        return jnp.concatenate(tiles, axis=1)

    head_shape = (LANES, q_cols)
    head_map = (
        lax.broadcasted_iota(jnp.int32, head_shape, 0) % heads
        == lax.broadcasted_iota(jnp.int32, head_shape, 1) // head_size
    ).astype(f32).astype(bf16)

    new_key = (row_scale * total[:, q_cols : q_cols + k_pad]).astype(bf16).astype(f32)
    new_value = (row_scale * total[:, q_cols + k_pad : q_cols + 2 * k_pad]).astype(bf16)
    product = query_ref[me].astype(f32) * grouped(new_key, q_cols)
    coarse = product.astype(bf16)
    fine = (product - coarse.astype(f32)).astype(bf16)
    new_score = sum(
        lax.dot_general(part, head_map, (((1,), (1,)), ((), ())), preferred_element_type=f32)
        for part in (coarse, fine)
    )
    gate = pltpu.roll(row_scale * misc, (LANES - my_tp * heads) % LANES, 1) + bias_pad_ref[...]
    log_gate = jnp.minimum(gate, 0.0) - jnp.log1p(jnp.exp(-jnp.abs(gate)))
    new_ref[me, :, :k_pad] = new_value.astype(f32)
    new_ref[me, :, k_pad:] = jnp.where(
        part_lane < heads, new_score * inv_root, pltpu.roll(log_gate, heads, 1)
    )

    def new_copy(source, target):
        return pltpu.make_async_remote_copy(
            src_ref=new_ref.at[source],
            dst_ref=new_ref.at[source],
            send_sem=new_send.at[target],
            recv_sem=new_recv.at[source],
            device_id={"kv": target},
            device_id_type=MESH,
        )

    for step in reversed(range(1, n_kv)):
        new_copy(me, flip(me, step, n_kv)).start()

    def part_copy(source, block, target):
        return pltpu.make_async_remote_copy(
            src_ref=part_ref.at[source, block],
            dst_ref=part_ref.at[source, block],
            send_sem=part_send.at[block, target],
            recv_sem=part_recv.at[block, source],
            device_id={"kv": target},
            device_id_type=MESH,
        )

    tall_row = lax.broadcasted_iota(jnp.int32, (tall, LANES), 0)
    tall_lane = lane_of((tall, LANES))
    stat_kind = (tall_lane % segment) // heads

    def spread(owner):
        query = query_ref[owner].astype(f32) * inv_root
        for at in range(0, q_cols, LANES):
            straight = query[:, at : at + LANES]
            turned = pltpu.roll(straight, head_size, 1)
            for half in range(2):
                low, high = (straight, turned) if half == 0 else (turned, straight)
                head = at // head_size + half
                wide_ref[pl.ds(head, mine, stride=heads), :] = jnp.where(
                    even_row, jnp.where(low_half, low, 0.0), jnp.where(low_half, 0.0, high)
                )
        wide = wide_ref[...]
        return jnp.concatenate(
            [
                jnp.where(tall_row // (2 * heads) == pair, wide, 0.0)
                for pair in range(pairs)
            ],
            axis=1,
        ).astype(bf16)

    def packed(owner, side, at):
        inside = slice(at, at + chunk_cols)
        return jnp.concatenate(
            [cache_ref[owner * mine + 2 * pair + side, inside, :] for pair in range(pairs)],
            axis=1,
        )

    def score(owner, queries, at):
        part = lax.dot_general(
            queries,
            packed(owner, 0, at),
            (((1,), (1,)), ((), ())),
            preferred_element_type=f32,
        )
        part = part + jnp.concatenate(
            [shift_ref[owner * mine + i, :, at : at + chunk_cols] for i in range(mine)], axis=0
        )
        score_ref[:, at : at + chunk_cols] = part
        return part

    def weigh(owner, peak, sums, values, at):
        weight = jnp.exp(score_ref[:, at : at + chunk_cols] - peak)
        values = values + jnp.dot(
            weight.astype(bf16), packed(owner, 1, at), preferred_element_type=f32
        )
        return sums + weight, values

    def set_peak(peak):
        peak_ref[...] = jnp.broadcast_to(jnp.max(peak, axis=1, keepdims=True), (tall, LANES))

    def begin(owner):
        queries = spread(owner)
        peak = None
        for at in chunks:
            part = score(owner, queries, at)
            peak = part if peak is None else jnp.maximum(peak, part)
        set_peak(peak)

    def finish(owner, after):
        queries = None if after is None else spread(after)
        block_peak = peak_ref[...]
        column = block_peak[:, :1]
        sums = jnp.zeros((tall, chunk_cols), f32)
        values = jnp.zeros((tall, pairs * LANES), f32)
        peak = None
        for at in chunks:
            sums, values = weigh(owner, column, sums, values, at)
            if after is not None:
                part = score(after, queries, at)
                peak = part if peak is None else jnp.maximum(peak, part)
        if after is not None:
            set_peak(peak)
        block_sum = jnp.sum(sums, axis=1, keepdims=True)
        value_ref[...] = jnp.concatenate(
            [
                values[
                    pair * 2 * heads : (pair + 1) * 2 * heads, pair * LANES : (pair + 1) * LANES
                ]
                for pair in range(pairs)
            ],
            axis=0,
        )
        last = jnp.concatenate([last_ref[owner * mine + i] for i in range(mine)], axis=0)
        stat_ref[...] = jnp.where(
            stat_kind == 0, block_peak, jnp.where(stat_kind == 1, block_sum, last)
        )
        stats = jnp.zeros((mine, LANES), f32)
        held = None
        for head in range(heads):
            inside = pl.ds(head, mine, stride=heads)
            stats = jnp.where(part_lane % heads == head, stat_ref[inside, :], stats)
            straight = value_ref[inside, :]
            turned = pltpu.roll(straight, head_size, 1)
            if head % 2 == 0:
                held = jnp.where(even_row, turned, straight)
            else:
                at = (head // 2) * LANES
                part_ref[me, owner, :, at : at + LANES] = jnp.where(
                    low_half, held, jnp.where(even_row, straight, turned)
                ).astype(bf16)
        coarse = stats.astype(bf16).astype(f32)
        medium = (stats - coarse).astype(bf16).astype(f32)
        fine = stats - coarse - medium
        part_ref[me, owner, :, q_cols:] = jnp.where(
            part_lane < segment, coarse, jnp.where(part_lane < 2 * segment, medium, fine)
        ).astype(bf16)
        for step in reversed(range(1, n_kv)):
            part_copy(me, owner, flip(me, step, n_kv)).start()

    begin(me)
    finish(me, None)
    first = flip(me, 1, n_kv)
    ag1_copy(first, me).wait_recv()
    begin(first)

    def attend(step, carry):
        owner, after = flip(me, step, n_kv), flip(me, step + 1, n_kv)
        ag1_copy(after, me).wait_recv()
        finish(owner, after)
        return carry

    lax.fori_loop(1, n_kv - 1, attend, 0)
    finish(flip(me, n_kv - 1, n_kv), None)

    def slot(place):
        return slice(place * mine, (place + 1) * mine)

    for place in range(n_kv):
        other = flip(me, place, n_kv)
        if place > 0:
            new_copy(other, me).wait_recv()
        fresh_ref[slot(place), :] = new_ref[other]
    loads[5].wait()
    for step in range(n_kv):
        for place in range(n_kv):
            source = flip(me, place, n_kv)
            block = flip(me, place ^ step, n_kv)
            if place > 0:
                part_copy(source, block, me).wait_recv()
            gathered_ref[place, slot(place ^ step), :] = part_ref[source, block].astype(f32)

    row_lane = lane_of((rows, LANES))
    fresh = fresh_ref[:, k_pad:]
    stats = []
    for place in range(n_kv):
        stat = gathered_ref[place, :, q_cols:]
        stat = stat + pltpu.roll(stat, LANES - segment, 1) + pltpu.roll(stat, LANES - 2 * segment, 1)
        stats.append(stat)
    last = stats[0]
    for stat in stats[1:]:
        last = last + stat
    cum_query = pltpu.roll(last, LANES - 2 * heads, 1) + pltpu.roll(fresh, LANES - heads, 1)
    new_biased = fresh - cum_query
    peak = new_biased
    for stat in stats:
        peak = jnp.maximum(peak, stat)
    new_weight = jnp.exp(new_biased - peak)
    weight_sum = new_weight
    factors = []
    for stat in stats:
        factor = jnp.exp(stat - peak)
        weight_sum = weight_sum + factor * pltpu.roll(stat, LANES - heads, 1)
        factors.append(factor)
    factors.append(new_weight.astype(bf16).astype(f32))
    log_weight = peak + jnp.log(weight_sum) + cum_query
    scales = []
    for factor in factors:
        scale = factor / weight_sum
        coarse = scale.astype(bf16).astype(f32)
        fine = pltpu.roll(scale - coarse, heads, 1)
        scales.append(
            jnp.where(
                row_lane < heads, coarse, jnp.where(row_lane < 2 * heads, fine, 0.0)
            ).astype(bf16)
        )
    attended = jnp.zeros((rows, q_cols), f32)
    for place, scale in enumerate(scales):
        wide = jnp.dot(scale, head_map, preferred_element_type=f32)
        if place < n_kv:
            attended = attended + wide * gathered_ref[place, :, :q_cols]
        else:
            attended = attended + wide * grouped(fresh_ref[:, :k_pad], q_cols)
    for place in range(n_kv):
        order_ref[flip(me, place, n_kv), :, :q_cols] = attended[slot(place)]
        order_ref[flip(me, place, n_kv), :, q_cols:] = log_weight[slot(place)]
    for owner in range(n_kv):
        fresh_ref[slot(owner), :] = jnp.concatenate(
            [order_ref[owner, :, q_cols:]] * (k_pad // LANES + 1), axis=1
        )
        wide_rows_ref[slot(owner), :] = order_ref[owner, :, :q_cols]
    tp_ref[my_tp] = jnp.dot(
        wide_rows_ref[...].astype(bf16), w_out_ref[...], preferred_element_type=f32
    ).astype(bf16)

    def tp_copy(source, target):
        return pltpu.make_async_remote_copy(
            src_ref=tp_ref.at[source],
            dst_ref=tp_ref.at[source],
            send_sem=tp_send.at[target],
            recv_sem=tp_recv.at[source],
            device_id={"tp": target},
            device_id_type=MESH,
        )

    for step in reversed(range(1, n_tp)):
        tp_copy(my_tp, flip(my_tp, step, n_tp)).start()

    log_ref[...] = fresh_ref[:, :heads]

    def settle(step, carry):
        other = flip(me, step, n_kv)
        rs1_copy(me, other).wait_send()
        ag1_copy(me, other).wait_send()
        new_copy(me, other).wait_send()
        for block in range(n_kv):
            part_copy(me, block, other).wait_send()
        return carry

    lax.fori_loop(1, n_kv, settle, 0)
    for step in range(1, n_tp):
        tp_copy(flip(my_tp, step, n_tp), my_tp).wait_recv()
    mixed = tp_ref[0].astype(f32)
    for source in range(1, n_tp):
        mixed = mixed + tp_ref[source].astype(f32)
    mixed_ref[...] = mixed.astype(bf16)
    for step in range(1, n_tp):
        tp_copy(my_tp, flip(my_tp, step, n_tp)).wait_send()


def shards(
    tokens,
    norm_gain,
    w_query,
    w_key,
    w_value,
    forget_weight,
    forget_bias,
    kv_cache,
    cum_gates,
    lengths,
    w_out,
):
    n_kv, n_tp = lax.axis_size("kv"), lax.axis_size("tp")
    rows, cols = tokens.shape
    span, kv_local, entry = kv_cache.shape[1:]
    heads = cum_gates.shape[1]
    q_cols, k_cols = w_query.shape[1], w_key.shape[1]
    k_pad = -(-k_cols // LANES) * LANES
    wide = q_cols + 2 * k_pad + LANES
    mine = rows // n_kv
    out_cols = w_out.shape[1]
    f32, bf16 = jnp.float32, jnp.bfloat16
    vmem = pl.BlockSpec(memory_space=pltpu.VMEM)
    smem = pl.BlockSpec(memory_space=pltpu.SMEM)
    hbm = pl.BlockSpec(memory_space=pl.ANY)
    dma = pltpu.SemaphoreType.DMA
    tall = (mine * heads, LANES)
    return pl.pallas_call(
        functools.partial(kernel, n_kv, n_tp),
        out_shape=(
            pltpu.VMEM((rows, out_cols), bf16),
            pltpu.VMEM((rows, heads), f32),
        ),
        in_specs=[vmem, vmem, vmem, smem] + [hbm] * 7,
        out_specs=(vmem, vmem),
        scratch_shapes=[
            pltpu.VMEM(w_query.shape, bf16),
            pltpu.VMEM(w_key.shape, bf16),
            pltpu.VMEM(w_value.shape, bf16),
            pltpu.VMEM((LANES, cols), bf16),
            pltpu.VMEM((rows, span * kv_local, entry), bf16),
            pltpu.VMEM(cum_gates.shape, f32),
            pltpu.VMEM(w_out.shape, bf16),
            pltpu.VMEM((rows, heads, span * kv_local), f32),
            pltpu.VMEM((rows, heads, LANES), f32),
            pltpu.VMEM((n_kv, mine, wide), bf16),
            pltpu.VMEM((n_kv, mine, wide), bf16),
            pltpu.VMEM((n_kv, mine, q_cols), bf16),
            pltpu.VMEM((n_kv, mine, k_pad + LANES), f32),
            pltpu.VMEM((1, LANES), f32),
            pltpu.VMEM(tall, f32),
            pltpu.VMEM((mine * heads, span * kv_local), f32),
            pltpu.VMEM(tall, f32),
            pltpu.VMEM(tall, f32),
            pltpu.VMEM(tall, f32),
            pltpu.VMEM((n_kv, n_kv, mine, q_cols + LANES), bf16),
            pltpu.VMEM((n_kv, rows, q_cols + LANES), f32),
            pltpu.VMEM((rows, k_pad + LANES), f32),
            pltpu.VMEM((n_kv, mine, q_cols + LANES), f32),
            pltpu.VMEM((rows, q_cols), f32),
            pltpu.VMEM((n_tp, rows, out_cols), bf16),
            dma((6,)),
            dma((n_kv,)),
        ]
        + [dma((n_kv,))] * 6
        + [dma((n_kv, n_kv))] * 2
        + [dma((n_tp,))] * 2,
        compiler_params=pltpu.CompilerParams(
            collective_id=0, has_side_effects=True, vmem_limit_bytes=56 * 1024 * 1024
        ),
    )(
        tokens,
        norm_gain.reshape(1, cols),
        forget_bias.reshape(1, heads),
        lengths,
        w_query,
        w_key,
        w_value,
        forget_weight.T,
        kv_cache.reshape(rows, span * kv_local, entry),
        cum_gates,
        w_out,
    )


def solution(mesh):
    placed = (
        P(None, "kv"),
        P("kv"),
        P("kv", "tp"),
        P("kv", "tp"),
        P("kv", "tp"),
        P(),
        P("tp"),
        P(None, "kv", "tp", None),
        P(None, "tp", "kv"),
        P(),
        P("tp", "kv"),
    )
    return jax.shard_map(
        shards,
        mesh=mesh,
        in_specs=placed,
        out_specs=(P(None, "kv"), P(None, "tp")),
        check_vma=False,
    )
```

time: 37.1 us -> 44.4 us (1.20)
  Pallas kernels: 35 us -> 42.2 us
    pallas_call x1, Pallas kernels: 35 us -> 42.2 us  [shards(): pl.pallas_call(functools.partial(kernel, n_kv, n_tp), out_shape=(pltpu.VM...]
where the time goes in v1:
time: 44.4 us; the launch traced here: 44.2 us
  Pallas kernels  42.2 us (95%)
  local copies, waits for them, and re-layouts  1.28 us (3%)
  between operations  0.64 us (1%)
    pallas_call x1, Pallas kernels, shards(): pl.pallas_call(functools.partial(kernel, n_kv, n_tp), out_shape=(pltpu.VM...  42.2 us

profile of v1, /device:TPU:0, one launch (start us, length us, event | category | flops | bytes accessed | tf_op | source)
XLA Modules:
  0.0 44.2 jit_solution(2110649776131427678)
XLA Ops:
  0.6 42.2 %shard_map.122 = (bf16[32,512]{1,0:T(8,128)(2,1)S(1)}, f32[32,8]{1,0:T(8,128)S(1)}) custom-call(bf16[32,512]{1,0:T(8,128)(2,1)} %tokens_ref.1, f32[1,512]{1,0:T(1,128)} %bitcast.6, f32[1,8]{1,0:T(1,128)} %bitcast.7, s32[32]{0:T(128)} %lengths_ref.1, bf16[512,512]{1,0:T(8,128)(2,1)} %w_query_hbm.1, bf16[512,128]{1,0:T(8,128)(2,1)} %w_key_hbm.1, ...), custom_call_target="tpu_custom_call" | custom-call | tf_op jit(solution)/shard_map/pallas_call | solution.py:577
  42.9 0.6 %copy.15 = bf16[32,512]{1,0:T(8,128)(2,1)} copy(bf16[32,512]{1,0:T(8,128)(2,1)S(1)} %get-tuple-element.4) | data formatting | bytes 65536
  43.5 0.7 %copy.13 = f32[32,8]{0,1:T(8,128)} copy(f32[32,8]{1,0:T(8,128)S(1)} %get-tuple-element.3) | data formatting | bytes 2048 | tf_op jit(solution)/shard_map/pallas_call | solution.py:577

commit v2 on v1

v2 whole, which is shorter than its diff:
```python
import functools
import jax
import jax.numpy as jnp
from jax import lax
from jax.experimental import pallas as pl
from jax.experimental.pallas import tpu as pltpu
from jax.sharding import PartitionSpec as P

norm_eps = 1e-05
masked_floor = -1e30
LANES = 128
MESH = pl.DeviceIdType.MESH


def flip(index, step, count):
    out = index
    bit = 1
    while bit < count:
        out = out + bit * ((step // bit) % 2) * (1 - 2 * ((index // bit) % 2))
        bit *= 2
    return out


def lane_of(shape):
    return lax.broadcasted_iota(jnp.int32, shape, len(shape) - 1)


def kernel(
    n_kv,
    n_tp,
    tokens_hbm,
    gain_hbm,
    bias_hbm,
    lengths_hbm,
    w_query_hbm,
    w_key_hbm,
    w_value_hbm,
    gate_hbm,
    cache_hbm,
    cum_hbm,
    w_out_hbm,
    mixed_ref,
    log_ref,
    tokens_ref,
    gain_ref,
    bias_ref,
    lengths_ref,
    w_query_ref,
    w_key_ref,
    w_value_ref,
    gate_ref,
    cache_ref,
    cum_ref,
    w_out_ref,
    shift_ref,
    last_ref,
    proj_ref,
    rs1_ref,
    query_ref,
    new_ref,
    bias_pad_ref,
    wide_ref,
    score_ref,
    peak_ref,
    value_ref,
    stat_ref,
    part_ref,
    gathered_ref,
    fresh_ref,
    order_ref,
    wide_rows_ref,
    tp_ref,
    weight_sems,
    cache_sems,
    rs1_send,
    rs1_recv,
    ag1_send,
    ag1_recv,
    new_send,
    new_recv,
    part_send,
    part_recv,
    tp_send,
    tp_recv,
):
    f32, bf16 = jnp.float32, jnp.bfloat16
    me = lax.axis_index("kv")
    my_tp = lax.axis_index("tp")
    rows, cols = tokens_ref.shape
    heads = cum_ref.shape[1]
    span = cum_ref.shape[2]
    entries = cache_ref.shape[1]
    kv_local = entries // span
    group = heads // kv_local
    head_size = LANES // 2
    all_heads = gate_hbm.shape[0]
    mine = rows // n_kv
    pairs = mine // 2
    q_cols = w_query_ref.shape[1]
    k_cols = w_key_ref.shape[1]
    k_pad = -(-k_cols // LANES) * LANES
    model_width = cols * n_kv
    inv_root = head_size ** (-0.5)
    chunk_cols = 2 * LANES
    chunks = range(0, entries, chunk_cols)
    segment = LANES // 4

    offset = pl.multiple_of(me * cols, cols)
    loads = [
        pltpu.make_async_copy(src, dst, weight_sems.at[i])
        for i, (src, dst) in enumerate(
            [
                (tokens_hbm, tokens_ref),
                (gain_hbm, gain_ref),
                (w_query_hbm, w_query_ref),
                (w_key_hbm, w_key_ref),
                (w_value_hbm, w_value_ref),
                (gate_hbm.at[:, pl.ds(offset, cols)], gate_ref.at[pl.ds(0, all_heads)]),
                (bias_hbm, bias_ref),
                (lengths_hbm, lengths_ref),
                (cum_hbm, cum_ref),
                (w_out_hbm, w_out_ref),
            ]
        )
    ]
    barrier = pltpu.get_barrier_semaphore()
    for step in range(1, n_kv):
        pl.semaphore_signal(
            barrier, inc=1, device_id={"kv": flip(me, step, n_kv)}, device_id_type=MESH
        )
    for step in range(1, n_tp):
        pl.semaphore_signal(
            barrier, inc=1, device_id={"tp": flip(my_tp, step, n_tp)}, device_id_type=MESH
        )
    for load in loads[:9]:
        load.start()

    def cache_load(owner):
        at = pl.ds(owner * mine, mine)
        return pltpu.make_async_copy(cache_hbm.at[at], cache_ref.at[at], cache_sems.at[owner])

    gate_ref[all_heads:, :] = jnp.zeros((LANES - all_heads, cols), bf16)
    bias_pad_ref[...] = jnp.zeros_like(bias_pad_ref)
    for load in loads[:2]:
        load.wait()
    tokens_f = tokens_ref[...].astype(f32)
    squares = jnp.sum(tokens_f * tokens_f, axis=1, keepdims=True)
    normed = (tokens_f * gain_ref[...]).astype(bf16)
    for load in loads[2:8]:
        load.wait()
    for step in range(n_kv):
        cache_load(flip(me, step, n_kv)).start()
    loads[9].start()
    bias_pad_ref[:, 0:heads] = bias_ref[...]
    pieces = [jnp.dot(normed, w_query_ref[...], preferred_element_type=f32)]
    for w_ref in (w_key_ref, w_value_ref):
        piece = jnp.dot(normed, w_ref[...], preferred_element_type=f32)
        if k_pad > k_cols:
            piece = jnp.concatenate([piece, jnp.zeros((rows, k_pad - k_cols), f32)], axis=1)
        pieces.append(piece)
    gates = lax.dot_general(
        normed, gate_ref[...], (((1,), (1,)), ((), ())), preferred_element_type=f32
    )
    pieces.append(jnp.where(lane_of(gates.shape) == all_heads, squares, gates))
    at = 0
    for piece in pieces:
        for owner in range(n_kv):
            proj_ref[owner, :, at : at + piece.shape[1]] = piece[
                owner * mine : (owner + 1) * mine
            ].astype(bf16)
        at += piece.shape[1]

    everyone = pl.ds(0, n_kv - 1)

    def rs1_copy(source, target):
        return pltpu.make_async_remote_copy(
            src_ref=proj_ref.at[target],
            dst_ref=rs1_ref.at[source],
            send_sem=rs1_send.at[0],
            recv_sem=rs1_recv.at[0],
            device_id={"kv": target},
            device_id_type=MESH,
        )

    def rs1_all():
        return pltpu.make_async_remote_copy(
            src_ref=proj_ref.at[everyone],
            dst_ref=rs1_ref.at[everyone],
            send_sem=rs1_send.at[0],
            recv_sem=rs1_recv.at[0],
            device_id={"kv": flip(me, 1, n_kv)},
            device_id_type=MESH,
        )

    pl.semaphore_wait(barrier, n_kv + n_tp - 2)
    for step in reversed(range(1, n_kv)):
        rs1_copy(me, flip(me, step, n_kv)).start()

    loads[8].wait()
    tile = (heads, LANES)
    lane = lane_of(tile)
    own_column = (lane % kv_local) == (lax.broadcasted_iota(jnp.int32, tile, 0) // group)

    def prepare(row, carry):
        length = lengths_ref[row] - me * span
        last = jnp.zeros(tile, f32)
        for chunk in range(span // LANES):
            cum = cum_ref[row, :, chunk * LANES : (chunk + 1) * LANES]
            place = lane + chunk * LANES
            shift = jnp.where(place < length, -cum, masked_floor)
            last = last + jnp.where(place == length - 1, cum, 0.0)
            for part in range(kv_local):
                if kv_local == 1:
                    spread = shift
                else:
                    pick = lane // kv_local + part * (LANES // kv_local)
                    spread = jnp.take_along_axis(shift, pick, axis=1)
                    spread = jnp.where(own_column, spread, masked_floor)
                at = (chunk * kv_local + part) * LANES
                shift_ref[row, :, at : at + LANES] = spread
        last_ref[row] = jnp.broadcast_to(jnp.sum(last, axis=1, keepdims=True), tile)
        return carry

    lax.fori_loop(0, rows, prepare, 0, unroll=4)

    total = proj_ref[me].astype(f32)
    rs1_all().wait_recv()
    for step in range(1, n_kv):
        total = total + rs1_ref[flip(me, step, n_kv)].astype(f32)
    misc = total[:, q_cols + 2 * k_pad :]
    part_lane = lane_of((mine, LANES))
    total_sq = jnp.sum(jnp.where(part_lane == all_heads, misc, 0.0), axis=1, keepdims=True)
    row_scale = lax.rsqrt(total_sq / model_width + norm_eps)
    query_ref[me] = (row_scale * total[:, :q_cols]).astype(bf16)

    def ag1_copy(source, target):
        return pltpu.make_async_remote_copy(
            src_ref=query_ref.at[source],
            dst_ref=query_ref.at[source],
            send_sem=ag1_send.at[0],
            recv_sem=ag1_recv.at[source],
            device_id={"kv": target},
            device_id_type=MESH,
        )

    for step in reversed(range(1, n_kv)):
        ag1_copy(me, flip(me, step, n_kv)).start()

    low_half = part_lane < head_size
    even_row = lax.broadcasted_iota(jnp.int32, (mine, LANES), 0) % 2 == 0

    def grouped(values, width):
        tiles = []
        for at in range(0, width, LANES):
            halves = []
            for half in range(2):
                source = (at // head_size + half) // group
                found = values[:, (source // 2) * LANES : (source // 2 + 1) * LANES]
                if source % 2 != half:
                    found = pltpu.roll(found, head_size, 1)
                halves.append(found)
            low = lane_of(halves[0].shape) < head_size
            tiles.append(jnp.where(low, halves[0], halves[1]))
        return jnp.concatenate(tiles, axis=1)

    head_shape = (LANES, q_cols)
    head_map = (
        lax.broadcasted_iota(jnp.int32, head_shape, 0) % heads
        == lax.broadcasted_iota(jnp.int32, head_shape, 1) // head_size
    ).astype(f32).astype(bf16)

    new_key = (row_scale * total[:, q_cols : q_cols + k_pad]).astype(bf16).astype(f32)
    new_value = (row_scale * total[:, q_cols + k_pad : q_cols + 2 * k_pad]).astype(bf16)
    product = query_ref[me].astype(f32) * grouped(new_key, q_cols)
    coarse = product.astype(bf16)
    fine = (product - coarse.astype(f32)).astype(bf16)
    new_score = sum(
        lax.dot_general(part, head_map, (((1,), (1,)), ((), ())), preferred_element_type=f32)
        for part in (coarse, fine)
    )
    gate = pltpu.roll(row_scale * misc, (LANES - my_tp * heads) % LANES, 1) + bias_pad_ref[...]
    log_gate = jnp.minimum(gate, 0.0) - jnp.log1p(jnp.exp(-jnp.abs(gate)))
    new_ref[me, :, :k_pad] = new_value.astype(f32)
    new_ref[me, :, k_pad:] = jnp.where(
        part_lane < heads, new_score * inv_root, pltpu.roll(log_gate, heads, 1)
    )

    def new_copy(source, target):
        return pltpu.make_async_remote_copy(
            src_ref=new_ref.at[source],
            dst_ref=new_ref.at[source],
            send_sem=new_send.at[0],
            recv_sem=new_recv.at[0],
            device_id={"kv": target},
            device_id_type=MESH,
        )

    def new_all():
        return pltpu.make_async_remote_copy(
            src_ref=new_ref.at[everyone],
            dst_ref=new_ref.at[everyone],
            send_sem=new_send.at[0],
            recv_sem=new_recv.at[0],
            device_id={"kv": flip(me, 1, n_kv)},
            device_id_type=MESH,
        )

    for step in reversed(range(1, n_kv)):
        new_copy(me, flip(me, step, n_kv)).start()

    early = n_kv - 2

    def part_copy(source, block, target, stage):
        return pltpu.make_async_remote_copy(
            src_ref=part_ref.at[source, block],
            dst_ref=part_ref.at[source, block],
            send_sem=part_send.at[0],
            recv_sem=part_recv.at[stage],
            device_id={"kv": target},
            device_id_type=MESH,
        )

    def part_all(count, stage):
        some = part_ref.at[pl.ds(0, count), everyone]
        return pltpu.make_async_remote_copy(
            src_ref=some,
            dst_ref=some,
            send_sem=part_send.at[0],
            recv_sem=part_recv.at[stage],
            device_id={"kv": flip(me, 1, n_kv)},
            device_id_type=MESH,
        )

    zeros = jnp.zeros((heads, LANES), f32)
    stat_kind = (lane % segment) // heads

    def cached(row_a, row_b, at):
        inside = slice(at, at + chunk_cols)
        return jnp.concatenate([cache_ref[row_a, inside, :], cache_ref[row_b, inside, :]], axis=1)

    def weigh(pair):
        peak = peak_ref[pair, :, :1]
        sums = jnp.zeros((2 * heads, chunk_cols), f32)
        weights = []
        for at in chunks:
            weight = jnp.exp(score_ref[pair, :, at : at + chunk_cols] - peak)
            sums = sums + weight
            weights.append(weight.astype(bf16))
        return weights, jnp.sum(sums, axis=1, keepdims=True), peak

    def score(owner, pair):
        first, second = 2 * pair, 2 * pair + 1
        row_a, row_b = owner * mine + first, owner * mine + second
        left = wide_ref[first * heads : (first + 1) * heads, :]
        right = wide_ref[second * heads : (second + 1) * heads, :]
        queries = jnp.concatenate(
            [
                jnp.concatenate([left, zeros], axis=1),
                jnp.concatenate([zeros, right], axis=1),
            ],
            axis=0,
        ).astype(bf16)
        peak = None
        for at in chunks:
            part = lax.dot_general(
                queries,
                cached(row_a, row_b, at),
                (((1,), (1,)), ((), ())),
                preferred_element_type=f32,
            )
            part = part + jnp.concatenate(
                [shift_ref[row_a, :, at : at + chunk_cols], shift_ref[row_b, :, at : at + chunk_cols]],
                axis=0,
            )
            score_ref[pair, :, at : at + chunk_cols] = part
            peak = part if peak is None else jnp.maximum(peak, part)
        peak_ref[pair] = jnp.broadcast_to(
            jnp.max(peak, axis=1, keepdims=True), (2 * heads, LANES)
        )

    def gather(owner, pair, weights, total_weight, peak):
        first, second = 2 * pair, 2 * pair + 1
        row_a, row_b = owner * mine + first, owner * mine + second
        values = jnp.zeros((2 * heads, chunk_cols), f32)
        for weight, at in zip(weights, chunks):
            values = values + jnp.dot(
                weight, cached(row_a, row_b, at), preferred_element_type=f32
            )
        for i, (place, row) in enumerate(((first, row_a), (second, row_b))):
            inside = slice(i * heads, (i + 1) * heads)
            place_rows = slice(place * heads, (place + 1) * heads)
            value_ref[place_rows, :] = values[inside, i * LANES : (i + 1) * LANES]
            stat_ref[place_rows, :] = jnp.where(
                stat_kind == 0,
                peak[inside],
                jnp.where(stat_kind == 1, total_weight[inside], last_ref[row]),
            )

    def ready(owner):
        cache_load(owner).wait()
        query = query_ref[owner].astype(f32) * inv_root
        for head in range(heads):
            at = (head // 2) * LANES
            found = query[:, at : at + LANES]
            if head % 2 == 1:
                found = pltpu.roll(found, head_size, 1)
            wide_ref[pl.ds(head, mine, stride=heads), :] = jnp.where(low_half, found, 0.0)

    def send(owner, stage):
        stats = jnp.zeros((mine, LANES), f32)
        held = None
        for head in range(heads):
            inside = pl.ds(head, mine, stride=heads)
            stats = jnp.where(part_lane % heads == head, stat_ref[inside, :], stats)
            found = value_ref[inside, :]
            if head % 2 == 0:
                held = pltpu.roll(found, head_size, 1)
            else:
                at = (head // 2) * LANES
                part_ref[me, owner, :, at : at + LANES] = jnp.where(low_half, held, found).astype(
                    bf16
                )
        coarse = stats.astype(bf16).astype(f32)
        medium = (stats - coarse).astype(bf16).astype(f32)
        fine = stats - coarse - medium
        part_ref[me, owner, :, q_cols:] = jnp.where(
            part_lane < segment, coarse, jnp.where(part_lane < 2 * segment, medium, fine)
        ).astype(bf16)
        for step in reversed(range(1, n_kv)):
            part_copy(me, owner, flip(me, step, n_kv), stage).start()

    ready(me)
    for pair in range(pairs):
        score(me, pair)
    for pair in range(pairs):
        gather(me, pair, *weigh(pair))
    send(me, 0)
    first = flip(me, 1, n_kv)
    ag1_copy(first, me).wait_recv()
    ready(first)
    for pair in range(pairs):
        score(first, pair)

    def attend(step, carry):
        owner, after = flip(me, step, n_kv), flip(me, step + 1, n_kv)
        ag1_copy(after, me).wait_recv()
        ready(after)
        for pair in range(pairs):
            weights = weigh(pair)
            score(after, pair)
            gather(owner, pair, *weights)
        send(owner, step // early)
        return carry

    lax.fori_loop(1, n_kv - 1, attend, 0)
    final = flip(me, n_kv - 1, n_kv)
    for pair in range(pairs):
        gather(final, pair, *weigh(pair))
    send(final, 1)

    def slot(place):
        return slice(place * mine, (place + 1) * mine)

    new_all().wait_recv()
    for place in range(n_kv):
        fresh_ref[slot(place), :] = new_ref[flip(me, place, n_kv)]
    loads[9].wait()
    for step in range(n_kv):
        if step == 0:
            part_all(early, 0).wait_recv()
        if step == early:
            part_all(n_kv - early, 1).wait_recv()
        for place in range(n_kv):
            source = flip(me, place, n_kv)
            block = flip(me, place ^ step, n_kv)
            gathered_ref[place, slot(place ^ step), :] = part_ref[source, block].astype(f32)

    row_lane = lane_of((rows, LANES))
    fresh = fresh_ref[:, k_pad:]
    stats = []
    for place in range(n_kv):
        stat = gathered_ref[place, :, q_cols:]
        stat = stat + pltpu.roll(stat, LANES - segment, 1) + pltpu.roll(stat, LANES - 2 * segment, 1)
        stats.append(stat)
    last = stats[0]
    for stat in stats[1:]:
        last = last + stat
    cum_query = pltpu.roll(last, LANES - 2 * heads, 1) + pltpu.roll(fresh, LANES - heads, 1)
    new_biased = fresh - cum_query
    peak = new_biased
    for stat in stats:
        peak = jnp.maximum(peak, stat)
    new_weight = jnp.exp(new_biased - peak)
    weight_sum = new_weight
    factors = []
    for stat in stats:
        factor = jnp.exp(stat - peak)
        weight_sum = weight_sum + factor * pltpu.roll(stat, LANES - heads, 1)
        factors.append(factor)
    factors.append(new_weight.astype(bf16).astype(f32))
    inverse = 1.0 / weight_sum
    scales = []
    for factor in factors:
        scale = factor * inverse
        coarse = scale.astype(bf16).astype(f32)
        fine = pltpu.roll(scale - coarse, heads, 1)
        scales.append(
            jnp.where(
                row_lane < heads, coarse, jnp.where(row_lane < 2 * heads, fine, 0.0)
            ).astype(bf16)
        )
    attended = jnp.zeros((rows, q_cols), f32)
    for place, scale in enumerate(scales):
        wide = jnp.dot(scale, head_map, preferred_element_type=f32)
        if place < n_kv:
            attended = attended + wide * gathered_ref[place, :, :q_cols]
        else:
            attended = attended + wide * grouped(fresh_ref[:, :k_pad], q_cols)
    for place in range(n_kv):
        order_ref[flip(me, place, n_kv), :, :q_cols] = attended[slot(place)]
    for owner in range(n_kv):
        wide_rows_ref[slot(owner), :] = order_ref[owner, :, :q_cols]
    tp_ref[my_tp] = jnp.dot(
        wide_rows_ref[...].astype(bf16), w_out_ref[...], preferred_element_type=f32
    ).astype(bf16)

    def tp_copy(source, target):
        return pltpu.make_async_remote_copy(
            src_ref=tp_ref.at[source],
            dst_ref=tp_ref.at[source],
            send_sem=tp_send.at[0],
            recv_sem=tp_recv.at[0],
            device_id={"tp": target},
            device_id_type=MESH,
        )

    def tp_all():
        some = tp_ref.at[pl.ds(0, n_tp - 1)]
        return pltpu.make_async_remote_copy(
            src_ref=some,
            dst_ref=some,
            send_sem=tp_send.at[0],
            recv_sem=tp_recv.at[0],
            device_id={"tp": flip(my_tp, 1, n_tp)},
            device_id_type=MESH,
        )

    for step in reversed(range(1, n_tp)):
        tp_copy(my_tp, flip(my_tp, step, n_tp)).start()

    log_weight = peak + jnp.log(weight_sum) + cum_query
    for place in range(n_kv):
        order_ref[flip(me, place, n_kv), :, q_cols:] = log_weight[slot(place)]
    for owner in range(n_kv):
        fresh_ref[slot(owner), k_pad:] = order_ref[owner, :, q_cols:]
    log_ref[...] = jnp.transpose(fresh_ref[:, k_pad:])[:heads]

    rs1_all().wait_send()
    pltpu.make_async_remote_copy(
        src_ref=query_ref.at[everyone],
        dst_ref=query_ref.at[everyone],
        send_sem=ag1_send.at[0],
        recv_sem=ag1_recv.at[0],
        device_id={"kv": flip(me, 1, n_kv)},
        device_id_type=MESH,
    ).wait_send()
    new_all().wait_send()
    part_all(n_kv, 0).wait_send()
    tp_all().wait_recv()
    mixed = tp_ref[0].astype(f32)
    for source in range(1, n_tp):
        mixed = mixed + tp_ref[source].astype(f32)
    mixed_ref[...] = mixed.astype(bf16)
    tp_all().wait_send()


def shards(
    tokens,
    norm_gain,
    w_query,
    w_key,
    w_value,
    forget_weight,
    forget_bias,
    kv_cache,
    cum_gates,
    lengths,
    w_out,
):
    n_kv, n_tp = lax.axis_size("kv"), lax.axis_size("tp")
    rows, cols = tokens.shape
    span, kv_local, entry = kv_cache.shape[1:]
    heads = cum_gates.shape[1]
    q_cols, k_cols = w_query.shape[1], w_key.shape[1]
    k_pad = -(-k_cols // LANES) * LANES
    wide = q_cols + 2 * k_pad + LANES
    mine = rows // n_kv
    out_cols = w_out.shape[1]
    f32, bf16 = jnp.float32, jnp.bfloat16
    vmem = pl.BlockSpec(memory_space=pltpu.VMEM)
    hbm = pl.BlockSpec(memory_space=pl.ANY)
    dma = pltpu.SemaphoreType.DMA
    tall = (mine * heads, LANES)
    mixed, log_weight = pl.pallas_call(
        functools.partial(kernel, n_kv, n_tp),
        out_shape=(
            pltpu.VMEM((rows, out_cols), bf16),
            pltpu.VMEM((heads, rows), f32),
        ),
        in_specs=[hbm] * 11,
        out_specs=(vmem, vmem),
        scratch_shapes=[
            pltpu.VMEM(tokens.shape, bf16),
            pltpu.VMEM((1, cols), f32),
            pltpu.VMEM((1, heads), f32),
            pltpu.SMEM(lengths.shape, jnp.int32),
            pltpu.VMEM(w_query.shape, bf16),
            pltpu.VMEM(w_key.shape, bf16),
            pltpu.VMEM(w_value.shape, bf16),
            pltpu.VMEM((LANES, cols), bf16),
            pltpu.VMEM((rows, span * kv_local, entry), bf16),
            pltpu.VMEM(cum_gates.shape, f32),
            pltpu.VMEM(w_out.shape, bf16),
            pltpu.VMEM((rows, heads, span * kv_local), f32),
            pltpu.VMEM((rows, heads, LANES), f32),
            pltpu.VMEM((n_kv, mine, wide), bf16),
            pltpu.VMEM((n_kv, mine, wide), bf16),
            pltpu.VMEM((n_kv, mine, q_cols), bf16),
            pltpu.VMEM((n_kv, mine, k_pad + LANES), f32),
            pltpu.VMEM((1, LANES), f32),
            pltpu.VMEM(tall, f32),
            pltpu.VMEM((mine // 2, 2 * heads, span * kv_local), f32),
            pltpu.VMEM((mine // 2, 2 * heads, LANES), f32),
            pltpu.VMEM(tall, f32),
            pltpu.VMEM(tall, f32),
            pltpu.VMEM((n_kv, n_kv, mine, q_cols + LANES), bf16),
            pltpu.VMEM((n_kv, rows, q_cols + LANES), f32),
            pltpu.VMEM((rows, k_pad + LANES), f32),
            pltpu.VMEM((n_kv, mine, q_cols + LANES), f32),
            pltpu.VMEM((rows, q_cols), f32),
            pltpu.VMEM((n_tp, rows, out_cols), bf16),
            dma((10,)),
            dma((n_kv,)),
            dma((1,)),
            dma((1,)),
            dma((1,)),
            dma((n_kv,)),
            dma((1,)),
            dma((1,)),
            dma((1,)),
            dma((2,)),
            dma((1,)),
            dma((1,)),
        ],
        compiler_params=pltpu.CompilerParams(
            collective_id=0, has_side_effects=True, vmem_limit_bytes=56 * 1024 * 1024
        ),
    )(
        tokens,
        norm_gain.reshape(1, cols),
        forget_bias.reshape(1, heads),
        lengths,
        w_query,
        w_key,
        w_value,
        forget_weight.T,
        kv_cache.reshape(rows, span * kv_local, entry),
        cum_gates,
        w_out,
    )
    return mixed, log_weight.T


def solution(mesh):
    placed = (
        P(None, "kv"),
        P("kv"),
        P("kv", "tp"),
        P("kv", "tp"),
        P("kv", "tp"),
        P(),
        P("tp"),
        P(None, "kv", "tp", None),
        P(None, "tp", "kv"),
        P(),
        P("tp", "kv"),
    )
    return jax.shard_map(
        shards,
        mesh=mesh,
        in_specs=placed,
        out_specs=(P(None, "kv"), P(None, "tp")),
        check_vma=False,
    )
```

time: 44.4 us -> 32.3 us (0.73)
  Pallas kernels: 42.2 us -> 30.3 us
    pallas_call x1, Pallas kernels: 42.2 us -> 30.3 us  [shards(): pl.pallas_call(functools.partial(kernel, n_kv, n_tp), out_shape=(pltpu.VM...]
    pallas_call x1 -> x0, local copies, waits for them, and re-layouts: 0.66 us -> none  [shards(): pl.pallas_call(functools.partial(kernel, n_kv, n_tp), out_shape=(pltpu.VM...]
    unnamed x1 -> x2, local copies, waits for them, and re-layouts: 0.62 us -> 1.21 us
where the time goes in v2:
time: 32.3 us; the launch traced here: 32.1 us
  Pallas kernels  30.3 us (94%)
  local copies, waits for them, and re-layouts  1.21 us (4%)
  between operations  0.64 us (2%)
    pallas_call x1, Pallas kernels, shards(): pl.pallas_call(functools.partial(kernel, n_kv, n_tp), out_shape=(pltpu.VM...  30.3 us
    unnamed x2, local copies, waits for them, and re-layouts  1.21 us

profile of v2, /device:TPU:0, one launch (start us, length us, event | category | flops | bytes accessed | tf_op | source)
XLA Modules:
  0.0 32.1 jit_solution(4882383678209634126)
XLA Ops:
  0.6 30.3 %shard_map.122 = (bf16[32,512]{1,0:T(8,128)(2,1)S(1)}, f32[8,32]{1,0:T(8,128)S(1)}) custom-call(bf16[32,512]{1,0:T(8,128)(2,1)} %tokens_hbm.1, f32[1,512]{1,0:T(1,128)} %bitcast.8, f32[1,8]{1,0:T(1,128)} %bitcast.9, s32[32]{0:T(128)} %lengths_hbm.1, bf16[512,512]{1,0:T(8,128)(2,1)} %w_query_hbm.1, bf16[512,128]{1,0:T(8,128)(2,1)} %w_key_hbm.1, ...), custom_call_target="tpu_custom_call" | custom-call | tf_op jit(solution)/shard_map/pallas_call | solution.py:604
  30.9 0.6 %copy.15 = bf16[32,512]{1,0:T(8,128)(2,1)} copy(bf16[32,512]{1,0:T(8,128)(2,1)S(1)} %get-tuple-element.6) | data formatting | bytes 65536
  31.5 0.6 %copy.16 = f32[32,8]{0,1:T(8,128)} copy(f32[32,8]{0,1:T(8,128)S(1)} %bitcast.5) | data formatting | bytes 2048

commit v3 on v2

--- a/solution.py
+++ b/solution.py
@@ -52,6 +52,7 @@
     cache_ref,
     cum_ref,
     w_out_ref,
+    turned_ref,
     shift_ref,
     last_ref,
     proj_ref,
@@ -192,10 +193,6 @@
             device_id_type=MESH,
         )
 
-    pl.semaphore_wait(barrier, n_kv + n_tp - 2)
-    for step in reversed(range(1, n_kv)):
-        rs1_copy(me, flip(me, step, n_kv)).start()
-
     loads[8].wait()
     tile = (heads, LANES)
     lane = lane_of(tile)
@@ -221,7 +218,47 @@
         last_ref[row] = jnp.broadcast_to(jnp.sum(last, axis=1, keepdims=True), tile)
         return carry
 
-    lax.fori_loop(0, rows, prepare, 0, unroll=4)
+    def prepare_four(i, carry):
+        for j in range(4):
+            prepare(4 * i + j, carry)
+        return carry
+
+    split = (rows // 8) * ((n_kv + n_kv // 4 - 1 - me) // (n_kv - n_kv // 8))
+    split = split + (rows // 8) * ((n_kv + n_kv // 2 - 1 - me) // (n_kv - n_kv // 8))
+    lax.fori_loop(0, split, prepare_four, 0)
+    pl.semaphore_wait(barrier, n_kv + n_tp - 2)
+    for step in reversed(range(1, n_kv)):
+        rs1_copy(me, flip(me, step, n_kv)).start()
+    lax.fori_loop(split, rows // 4, prepare_four, 0)
+
+    def cached(row_a, row_b, at):
+        inside = slice(at, at + chunk_cols)
+        return jnp.concatenate([cache_ref[row_a, inside, :], cache_ref[row_b, inside, :]], axis=1)
+
+    pick_shape = (LANES, 2 * LANES)
+    pick_row = lax.broadcasted_iota(jnp.int32, pick_shape, 0)
+    pick = (
+        lane_of(pick_shape) == pick_row + (pick_row // head_size) * head_size
+    ).astype(f32).astype(bf16)
+
+    def turn(step, carry):
+        owner = flip(me, step, n_kv)
+        cache_load(owner).wait()
+        for pair in range(pairs):
+            row = owner * mine + 2 * pair
+            for at in chunks:
+                turned_ref[step - 1, pair * LANES : (pair + 1) * LANES, at : at + chunk_cols] = (
+                    lax.dot_general(
+                        pick,
+                        cached(row, row + 1, at),
+                        (((1,), (1,)), ((), ())),
+                        preferred_element_type=f32,
+                    ).astype(bf16)
+                )
+        return carry
+
+    ahead = turned_ref.shape[0]
+    lax.fori_loop(1, ahead + 1, turn, 0)
 
     total = proj_ref[me].astype(f32)
     rs1_all().wait_recv()
@@ -332,23 +369,25 @@
         )
 
     zeros = jnp.zeros((heads, LANES), f32)
+    tall_pair = lax.broadcasted_iota(jnp.int32, (mine * heads, LANES), 0) // (2 * heads)
     stat_kind = (lane % segment) // heads
 
-    def cached(row_a, row_b, at):
-        inside = slice(at, at + chunk_cols)
-        return jnp.concatenate([cache_ref[row_a, inside, :], cache_ref[row_b, inside, :]], axis=1)
-
-    def weigh(pair):
-        peak = peak_ref[pair, :, :1]
+    def weigh(pair, buffer):
+        peak = peak_ref[buffer, pair, :, :1]
         sums = jnp.zeros((2 * heads, chunk_cols), f32)
         weights = []
         for at in chunks:
-            weight = jnp.exp(score_ref[pair, :, at : at + chunk_cols] - peak)
+            weight = jnp.exp(score_ref[buffer, pair, :, at : at + chunk_cols] - peak)
             sums = sums + weight
             weights.append(weight.astype(bf16))
         return weights, jnp.sum(sums, axis=1, keepdims=True), peak
 
-    def score(owner, pair):
+    def shifts(row, count, at):
+        return jnp.concatenate(
+            [shift_ref[row + i, :, at : at + chunk_cols] for i in range(count)], axis=0
+        )
+
+    def score(owner, pair, buffer):
         first, second = 2 * pair, 2 * pair + 1
         row_a, row_b = owner * mine + first, owner * mine + second
         left = wide_ref[first * heads : (first + 1) * heads, :]
@@ -368,15 +407,44 @@
                 (((1,), (1,)), ((), ())),
                 preferred_element_type=f32,
             )
-            part = part + jnp.concatenate(
-                [shift_ref[row_a, :, at : at + chunk_cols], shift_ref[row_b, :, at : at + chunk_cols]],
-                axis=0,
+            part = part + shifts(row_a, 2, at)
+            score_ref[buffer, pair, :, at : at + chunk_cols] = part
+            peak = part if peak is None else jnp.maximum(peak, part)
+        peak_ref[buffer, pair] = jnp.broadcast_to(
+            jnp.max(peak, axis=1, keepdims=True), (2 * heads, LANES)
+        )
+
+    def score_turned(step, buffer):
+        owner = flip(me, step, n_kv)
+        query = query_ref[owner].astype(f32) * inv_root
+        for head in range(heads):
+            at = (head // 2) * LANES
+            found = query[:, at : at + LANES]
+            other = pltpu.roll(found, head_size, 1)
+            low, high = (found, other) if head % 2 == 0 else (other, found)
+            wide_ref[pl.ds(head, mine, stride=heads), :] = jnp.where(
+                even_row, jnp.where(low_half, low, 0.0), jnp.where(low_half, 0.0, high)
             )
-            score_ref[pair, :, at : at + chunk_cols] = part
+        wide = wide_ref[...]
+        queries = jnp.concatenate(
+            [jnp.where(tall_pair == pair, wide, 0.0) for pair in range(pairs)], axis=1
+        ).astype(bf16)
+        peak = None
+        for at in chunks:
+            part = jnp.dot(
+                queries,
+                turned_ref[step - 1, :, at : at + chunk_cols],
+                preferred_element_type=f32,
+            )
+            part = part + shifts(owner * mine, mine, at)
+            for pair in range(pairs):
+                score_ref[buffer, pair, :, at : at + chunk_cols] = part[
+                    pair * 2 * heads : (pair + 1) * 2 * heads
+                ]
             peak = part if peak is None else jnp.maximum(peak, part)
-        peak_ref[pair] = jnp.broadcast_to(
-            jnp.max(peak, axis=1, keepdims=True), (2 * heads, LANES)
-        )
+        peak = jnp.broadcast_to(jnp.max(peak, axis=1, keepdims=True), (mine * heads, LANES))
+        for pair in range(pairs):
+            peak_ref[buffer, pair] = peak[pair * 2 * heads : (pair + 1) * 2 * heads]
 
     def gather(owner, pair, weights, total_weight, peak):
         first, second = 2 * pair, 2 * pair + 1
@@ -397,7 +465,6 @@
             )
 
     def ready(owner):
-        cache_load(owner).wait()
         query = query_ref[owner].astype(f32) * inv_root
         for head in range(heads):
             at = (head // 2) * LANES
@@ -429,33 +496,41 @@
         for step in reversed(range(1, n_kv)):
             part_copy(me, owner, flip(me, step, n_kv), stage).start()
 
+    cache_load(me).wait()
     ready(me)
     for pair in range(pairs):
-        score(me, pair)
+        score(me, pair, 0)
     for pair in range(pairs):
-        gather(me, pair, *weigh(pair))
+        gather(me, pair, *weigh(pair, 0))
     send(me, 0)
-    first = flip(me, 1, n_kv)
-    ag1_copy(first, me).wait_recv()
-    ready(first)
-    for pair in range(pairs):
-        score(first, pair)
+    ag1_copy(flip(me, 1, n_kv), me).wait_recv()
+    score_turned(1, 0)
+    for step in range(1, ahead):
+        ag1_copy(flip(me, step + 1, n_kv), me).wait_recv()
+        owner = flip(me, step, n_kv)
+        now, later = (step - 1) % 2, step % 2
+        score_turned(step + 1, later)
+        for pair in range(pairs):
+            gather(owner, pair, *weigh(pair, now))
+        send(owner, 0)
+    last_buffer = (ahead - 1) % 2
 
     def attend(step, carry):
         owner, after = flip(me, step, n_kv), flip(me, step + 1, n_kv)
+        cache_load(after).wait()
         ag1_copy(after, me).wait_recv()
         ready(after)
         for pair in range(pairs):
-            weights = weigh(pair)
-            score(after, pair)
+            weights = weigh(pair, last_buffer)
+            score(after, pair, last_buffer)
             gather(owner, pair, *weights)
         send(owner, step // early)
         return carry
 
-    lax.fori_loop(1, n_kv - 1, attend, 0)
+    lax.fori_loop(ahead, n_kv - 1, attend, 0)
     final = flip(me, n_kv - 1, n_kv)
     for pair in range(pairs):
-        gather(final, pair, *weigh(pair))
+        gather(final, pair, *weigh(pair, last_buffer))
     send(final, 1)
 
     def slot(place):
@@ -545,7 +620,7 @@
             device_id_type=MESH,
         )
 
-    for step in reversed(range(1, n_tp)):
+    for step in (2, 3, 1) if n_tp == 4 else reversed(range(1, n_tp)):
         tp_copy(my_tp, flip(my_tp, step, n_tp)).start()
 
     log_weight = peak + jnp.log(weight_sum) + cum_query
@@ -621,6 +696,7 @@
             pltpu.VMEM((rows, span * kv_local, entry), bf16),
             pltpu.VMEM(cum_gates.shape, f32),
             pltpu.VMEM(w_out.shape, bf16),
+            pltpu.VMEM((3, mine * (entry // 2), span * kv_local), bf16),
             pltpu.VMEM((rows, heads, span * kv_local), f32),
             pltpu.VMEM((rows, heads, LANES), f32),
             pltpu.VMEM((n_kv, mine, wide), bf16),
@@ -629,8 +705,8 @@
             pltpu.VMEM((n_kv, mine, k_pad + LANES), f32),
             pltpu.VMEM((1, LANES), f32),
             pltpu.VMEM(tall, f32),
-            pltpu.VMEM((mine // 2, 2 * heads, span * kv_local), f32),
-            pltpu.VMEM((mine // 2, 2 * heads, LANES), f32),
+            pltpu.VMEM((2, mine // 2, 2 * heads, span * kv_local), f32),
+            pltpu.VMEM((2, mine // 2, 2 * heads, LANES), f32),
             pltpu.VMEM(tall, f32),
             pltpu.VMEM(tall, f32),
             pltpu.VMEM((n_kv, n_kv, mine, q_cols + LANES), bf16),

time: 32.3 us -> 31 us (0.960)
  Pallas kernels: 30.3 us -> 29 us
    pallas_call x1, Pallas kernels: 30.3 us -> 29 us  [shards(): pl.pallas_call(functools.partial(kernel, n_kv, n_tp), out_shape=(pltpu.VM...]
where the time goes in v3:
time: 31 us; the launch traced here: 30.8 us
  Pallas kernels  29 us (94%)
  local copies, waits for them, and re-layouts  1.21 us (4%)
  between operations  0.64 us (2%)
    pallas_call x1, Pallas kernels, shards(): pl.pallas_call(functools.partial(kernel, n_kv, n_tp), out_shape=(pltpu.VM...  29 us
    unnamed x2, local copies, waits for them, and re-layouts  1.21 us

profile of v3, /device:TPU:0, one launch (start us, length us, event | category | flops | bytes accessed | tf_op | source)
XLA Modules:
  0.0 30.8 jit_solution(143026267673095327)
XLA Ops:
  0.6 29.0 %shard_map.122 = (bf16[32,512]{1,0:T(8,128)(2,1)S(1)}, f32[8,32]{1,0:T(8,128)S(1)}) custom-call(bf16[32,512]{1,0:T(8,128)(2,1)} %tokens_hbm.1, f32[1,512]{1,0:T(1,128)} %bitcast.8, f32[1,8]{1,0:T(1,128)} %bitcast.9, s32[32]{0:T(128)} %lengths_hbm.1, bf16[512,512]{1,0:T(8,128)(2,1)} %w_query_hbm.1, bf16[512,128]{1,0:T(8,128)(2,1)} %w_key_hbm.1, ...), custom_call_target="tpu_custom_call" | custom-call | tf_op jit(solution)/shard_map/pallas_call | solution.py:679
  29.6 0.6 %copy.15 = bf16[32,512]{1,0:T(8,128)(2,1)} copy(bf16[32,512]{1,0:T(8,128)(2,1)S(1)} %get-tuple-element.6) | data formatting | bytes 65536
  30.2 0.6 %copy.16 = f32[32,8]{0,1:T(8,128)} copy(f32[32,8]{0,1:T(8,128)S(1)} %bitcast.5) | data formatting | bytes 2048

commit v4 on v3

--- a/solution.py
+++ b/solution.py
@@ -149,7 +149,9 @@
     normed = (tokens_f * gain_ref[...]).astype(bf16)
     for load in loads[2:8]:
         load.wait()
-    for step in range(n_kv):
+    ahead = turned_ref.shape[0]
+    flight = 3
+    for step in range(1, flight + 1):
         cache_load(flip(me, step, n_kv)).start()
     loads[9].start()
     bias_pad_ref[:, 0:heads] = bias_ref[...]
@@ -198,7 +200,7 @@
     lane = lane_of(tile)
     own_column = (lane % kv_local) == (lax.broadcasted_iota(jnp.int32, tile, 0) // group)
 
-    def prepare(row, carry):
+    def prepare(row):
         length = lengths_ref[row] - me * span
         last = jnp.zeros(tile, f32)
         for chunk in range(span // LANES):
@@ -216,20 +218,12 @@
                 at = (chunk * kv_local + part) * LANES
                 shift_ref[row, :, at : at + LANES] = spread
         last_ref[row] = jnp.broadcast_to(jnp.sum(last, axis=1, keepdims=True), tile)
+
+    def prepare_block(step, carry):
+        owner = flip(me, step, n_kv)
+        for i in range(mine):
+            prepare(owner * mine + i)
         return carry
-
-    def prepare_four(i, carry):
-        for j in range(4):
-            prepare(4 * i + j, carry)
-        return carry
-
-    split = (rows // 8) * ((n_kv + n_kv // 4 - 1 - me) // (n_kv - n_kv // 8))
-    split = split + (rows // 8) * ((n_kv + n_kv // 2 - 1 - me) // (n_kv - n_kv // 8))
-    lax.fori_loop(0, split, prepare_four, 0)
-    pl.semaphore_wait(barrier, n_kv + n_tp - 2)
-    for step in reversed(range(1, n_kv)):
-        rs1_copy(me, flip(me, step, n_kv)).start()
-    lax.fori_loop(split, rows // 4, prepare_four, 0)
 
     def cached(row_a, row_b, at):
         inside = slice(at, at + chunk_cols)
@@ -241,9 +235,16 @@
         lane_of(pick_shape) == pick_row + (pick_row // head_size) * head_size
     ).astype(f32).astype(bf16)
 
+    def following(step):
+        place = step + flight
+        past = place // (ahead + 1)
+        beyond = place // (ahead + 2)
+        return place - past * (ahead + 1) + beyond * (ahead + 1) - beyond
+
     def turn(step, carry):
         owner = flip(me, step, n_kv)
         cache_load(owner).wait()
+        cache_load(flip(me, following(step), n_kv)).start()
         for pair in range(pairs):
             row = owner * mine + 2 * pair
             for at in chunks:
@@ -257,8 +258,18 @@
                 )
         return carry
 
-    ahead = turned_ref.shape[0]
-    lax.fori_loop(1, ahead + 1, turn, 0)
+    few = n_kv - n_kv // 8
+    ready_blocks = 3 * ((n_kv + n_kv // 2 - 1 - me) // few)
+    turned_blocks = 1 + (n_kv - 1 - me) // few + (n_kv + n_kv // 4 - 1 - me) // few
+    lax.fori_loop(0, ready_blocks, prepare_block, 0)
+    lax.fori_loop(1, turned_blocks, turn, 0)
+    pl.semaphore_wait(barrier, n_kv + n_tp - 2)
+    for step in reversed(range(1, n_kv)):
+        rs1_copy(me, flip(me, step, n_kv)).start()
+    lax.fori_loop(ready_blocks, 3, prepare_block, 0)
+    lax.fori_loop(turned_blocks, ahead + 1, turn, 0)
+    for place in range(ahead + flight + 1, n_kv + 1):
+        cache_load(flip(me, place - 1, n_kv)).start()
 
     total = proj_ref[me].astype(f32)
     rs1_all().wait_recv()
@@ -509,6 +520,7 @@
         ag1_copy(flip(me, step + 1, n_kv), me).wait_recv()
         owner = flip(me, step, n_kv)
         now, later = (step - 1) % 2, step % 2
+        prepare_block(step + 2, 0)
         score_turned(step + 1, later)
         for pair in range(pairs):
             gather(owner, pair, *weigh(pair, now))
@@ -519,6 +531,7 @@
         owner, after = flip(me, step, n_kv), flip(me, step + 1, n_kv)
         cache_load(after).wait()
         ag1_copy(after, me).wait_recv()
+        prepare_block(step + 2, 0)
         ready(after)
         for pair in range(pairs):
             weights = weigh(pair, last_buffer)
@@ -540,6 +553,20 @@
     for place in range(n_kv):
         fresh_ref[slot(place), :] = new_ref[flip(me, place, n_kv)]
     loads[9].wait()
+    row_lane = lane_of((rows, LANES))
+    fresh = fresh_ref[:, k_pad:]
+    fresh_gate = pltpu.roll(fresh, LANES - heads, 1)
+    fresh_values = grouped(fresh_ref[:, :k_pad], q_cols)
+    merge_shape = (LANES, 3 * LANES)
+    merge_row = lax.broadcasted_iota(jnp.int32, merge_shape, 0)
+    merge_place = merge_row % segment
+    merge_lane = lane_of(merge_shape)
+    merge_map = (
+        (merge_row < 3 * segment)
+        & (merge_place // heads == merge_lane // LANES)
+        & (merge_place % heads == merge_lane % LANES)
+    ).astype(f32).astype(bf16)
+    scale_map = jnp.concatenate([head_map, head_map], axis=0)
     for step in range(n_kv):
         if step == 0:
             part_all(early, 0).wait_recv()
@@ -550,47 +577,45 @@
             block = flip(me, place ^ step, n_kv)
             gathered_ref[place, slot(place ^ step), :] = part_ref[source, block].astype(f32)
 
-    row_lane = lane_of((rows, LANES))
-    fresh = fresh_ref[:, k_pad:]
-    stats = []
+    merged = jnp.dot(
+        jnp.concatenate(
+            [gathered_ref[place, :, q_cols:].astype(bf16) for place in range(n_kv)], axis=0
+        ),
+        merge_map,
+        preferred_element_type=f32,
+    )
+
+    def stat(place, kind):
+        return merged[place * rows : (place + 1) * rows, kind * LANES : (kind + 1) * LANES]
+
+    cum_query = fresh_gate
     for place in range(n_kv):
-        stat = gathered_ref[place, :, q_cols:]
-        stat = stat + pltpu.roll(stat, LANES - segment, 1) + pltpu.roll(stat, LANES - 2 * segment, 1)
-        stats.append(stat)
-    last = stats[0]
-    for stat in stats[1:]:
-        last = last + stat
-    cum_query = pltpu.roll(last, LANES - 2 * heads, 1) + pltpu.roll(fresh, LANES - heads, 1)
+        cum_query = cum_query + stat(place, 2)
     new_biased = fresh - cum_query
     peak = new_biased
-    for stat in stats:
-        peak = jnp.maximum(peak, stat)
+    for place in range(n_kv):
+        peak = jnp.maximum(peak, stat(place, 0))
     new_weight = jnp.exp(new_biased - peak)
     weight_sum = new_weight
     factors = []
-    for stat in stats:
-        factor = jnp.exp(stat - peak)
-        weight_sum = weight_sum + factor * pltpu.roll(stat, LANES - heads, 1)
+    for place in range(n_kv):
+        factor = jnp.exp(stat(place, 0) - peak)
+        weight_sum = weight_sum + factor * stat(place, 1)
         factors.append(factor)
     factors.append(new_weight.astype(bf16).astype(f32))
-    inverse = 1.0 / weight_sum
+    inverse = jnp.where(row_lane < heads, 1.0 / weight_sum, 0.0)
     scales = []
     for factor in factors:
-        scale = factor * inverse
-        coarse = scale.astype(bf16).astype(f32)
-        fine = pltpu.roll(scale - coarse, heads, 1)
-        scales.append(
-            jnp.where(
-                row_lane < heads, coarse, jnp.where(row_lane < 2 * heads, fine, 0.0)
-            ).astype(bf16)
-        )
-    attended = jnp.zeros((rows, q_cols), f32)
-    for place, scale in enumerate(scales):
-        wide = jnp.dot(scale, head_map, preferred_element_type=f32)
-        if place < n_kv:
-            attended = attended + wide * gathered_ref[place, :, :q_cols]
-        else:
-            attended = attended + wide * grouped(fresh_ref[:, :k_pad], q_cols)
+        scale = jnp.where(row_lane < heads, factor * inverse, 0.0)
+        coarse = scale.astype(bf16)
+        fine = (scale - coarse.astype(f32)).astype(bf16)
+        scales.append(jnp.concatenate([coarse, fine], axis=1))
+    wide = jnp.dot(jnp.concatenate(scales, axis=0), scale_map, preferred_element_type=f32)
+    attended = wide[n_kv * rows :] * fresh_values
+    for place in range(n_kv):
+        attended = attended + wide[place * rows : (place + 1) * rows] * (
+            gathered_ref[place, :, :q_cols]
+        )
     for place in range(n_kv):
         order_ref[flip(me, place, n_kv), :, :q_cols] = attended[slot(place)]
     for owner in range(n_kv):
@@ -696,7 +721,7 @@
             pltpu.VMEM((rows, span * kv_local, entry), bf16),
             pltpu.VMEM(cum_gates.shape, f32),
             pltpu.VMEM(w_out.shape, bf16),
-            pltpu.VMEM((3, mine * (entry // 2), span * kv_local), bf16),
+            pltpu.VMEM((4, mine * (entry // 2), span * kv_local), bf16),
             pltpu.VMEM((rows, heads, span * kv_local), f32),
             pltpu.VMEM((rows, heads, LANES), f32),
             pltpu.VMEM((n_kv, mine, wide), bf16),

time: 31 us -> 30.8 us (level)
  no operation moved by 1% of the time
where the time goes in v4:
time: 30.8 us; the launch traced here: 30.6 us
  Pallas kernels  28.8 us (94%)
  local copies, waits for them, and re-layouts  1.21 us (4%)
  between operations  0.64 us (2%)
    pallas_call x1, Pallas kernels, shards(): pl.pallas_call(functools.partial(kernel, n_kv, n_tp), out_shape=(pltpu.VM...  28.8 us
    unnamed x2, local copies, waits for them, and re-layouts  1.21 us

profile of v4, /device:TPU:0, one launch (start us, length us, event | category | flops | bytes accessed | tf_op | source)
XLA Modules:
  0.0 30.6 jit_solution(4550253720337090725)
XLA Ops:
  0.6 28.8 %shard_map.122 = (bf16[32,512]{1,0:T(8,128)(2,1)S(1)}, f32[8,32]{1,0:T(8,128)S(1)}) custom-call(bf16[32,512]{1,0:T(8,128)(2,1)} %tokens_hbm.1, f32[1,512]{1,0:T(1,128)} %bitcast.8, f32[1,8]{1,0:T(1,128)} %bitcast.9, s32[32]{0:T(128)} %lengths_hbm.1, bf16[512,512]{1,0:T(8,128)(2,1)} %w_query_hbm.1, bf16[512,128]{1,0:T(8,128)(2,1)} %w_key_hbm.1, ...), custom_call_target="tpu_custom_call" | custom-call | tf_op jit(solution)/shard_map/pallas_call | solution.py:704
  29.4 0.6 %copy.15 = bf16[32,512]{1,0:T(8,128)(2,1)} copy(bf16[32,512]{1,0:T(8,128)(2,1)S(1)} %get-tuple-element.6) | data formatting | bytes 65536
  30.0 0.6 %copy.16 = f32[32,8]{0,1:T(8,128)} copy(f32[32,8]{0,1:T(8,128)S(1)} %bitcast.5) | data formatting | bytes 2048
